TPU v7x, 32 devices: a whole 2x2x4 slice. The times are simulated.
32 devices in a mesh: fs: 16 (over z, y, x), tp: 2 (over core).
Axes of the slice: x: 2, y: 2, z: 4, core: 2. Of those that a mesh axis runs over, the one named last changes fastest.
Arguments:
- tokens: bfloat16 [3072, 2048], P('fs'), may hold values from -6 to 6
- route_ids: int32 [3072, 2], P('fs'), may hold values from 0 to 7, all different within a row; in each aligned block of 192 rows (0 to 191, 192 to 383, ...) at most 96 rows name the same one
- route_logits: float32 [3072, 2], P('fs'), may hold values from -6 to 6
- norm_gain: float32 [2048], P('fs'), may hold values from 0.1 to 1.9
- gate_weight: float32 [8, 2048, 2048], P(None, 'fs', 'tp'), may hold values from -0.125 to 0.125
- up_weight: float32 [8, 2048, 2048], P(None, 'fs', 'tp'), may hold values from -0.125 to 0.125
- down_weight: float32 [8, 2048, 2048], P(None, 'fs', 'tp'), may hold values from -0.125 to 0.125
Outputs:
- mixed: bfloat16 [3072, 2048], P('fs')
- gate_copies: bfloat16 [16, 2048, 2048], P('fs', None, 'tp')
- up_copies: bfloat16 [16, 2048, 2048], P('fs', None, 'tp')
- down_copies: bfloat16 [16, 2048, 2048], P('fs', None, 'tp')
Inputs may be any that keep to these rules, and one draw needn't show every extreme that they name: `route_ids`: each row names 2 different experts. Among the rows of one index of fs no expert is named by more than 96 rows, a bound that some of them reach.
All inputs are finite; a program needn't handle non-finite values.
Results may differ from a plain program's by a relative error of at most 0.014.
Values may be sent and summed in bfloat16 or wider, within the bound.
No kernel may reach another device: no remote copies, remote signals or barrier semaphores. Data moves between devices by JAX's collectives and lax.ppermute only.
A program may use at most 128 MiB of HBM per device.

v0:
```python
import jax
import jax.numpy as jnp
from jax import lax
from jax.sharding import PartitionSpec as P

CAP = 96


def body(tokens, route_ids, route_logits, norm_gain, gate_weight, up_weight, down_weight):
    experts = gate_weight.shape[0]
    fs_count = lax.axis_size("fs")
    copies = fs_count // experts
    per_peer = CAP // copies
    tok_rows = tokens.shape[0]
    width = tokens.shape[1]
    scaled_gain = norm_gain[None, :, None]
    gate_send = jnp.repeat((scaled_gain * gate_weight).astype(jnp.bfloat16), copies, axis=0)
    up_send = jnp.repeat((scaled_gain * up_weight).astype(jnp.bfloat16), copies, axis=0)
    down_send = jnp.repeat(down_weight.astype(jnp.bfloat16), copies, axis=0)
    gate_new, up_new, down_new = (
        lax.all_to_all(gate_send, "fs", split_axis=0, concat_axis=1, tiled=True),
        lax.all_to_all(up_send, "fs", split_axis=0, concat_axis=1, tiled=True),
        lax.all_to_all(down_send, "fs", split_axis=0, concat_axis=1, tiled=True),
    )
    values = tokens.astype(jnp.float32)
    center = jnp.mean(values, axis=1, keepdims=True)
    spread = jnp.mean(jnp.square(values - center), axis=1, keepdims=True)
    normed = ((values - center) * lax.rsqrt(spread + 1e-06)).astype(jnp.bfloat16)
    flat_ids = route_ids.reshape(-1)
    onehot_table = (flat_ids[:, None] == jnp.arange(experts, dtype=jnp.int32)[None, :]).astype(
        jnp.int32
    )
    before = jnp.cumsum(onehot_table, axis=0) - onehot_table
    order_rank = jnp.sum(before * onehot_table, axis=1)
    dest_flat = (flat_ids * copies + order_rank % copies) * per_peer + order_rank // copies
    owners = jnp.arange(flat_ids.shape[0], dtype=jnp.int32) // route_ids.shape[1]
    slot_token = jnp.full((experts * CAP,), tok_rows, jnp.int32).at[dest_flat].set(owners)
    padded = jnp.concatenate([normed, jnp.zeros((1, width), jnp.bfloat16)], axis=0)
    send_rows = padded[slot_token].reshape(fs_count, per_peer, width)
    gate_matrix = gate_new[0]
    up_matrix = up_new[0]
    col_count = width // lax.axis_size("tp")
    col_start = lax.axis_index("tp") * col_count
    own_cols = lax.dynamic_slice_in_dim(send_rows, col_start, col_count, 2)
    arrived = lax.all_to_all(own_cols, "fs", split_axis=0, concat_axis=0, tiled=True).reshape(
        -1, col_count
    )
    piece = lax.all_gather(arrived, "tp", axis=1, tiled=True)
    gate_act = jnp.dot(piece, gate_matrix, preferred_element_type=jnp.float32)
    up_act = jnp.dot(piece, up_matrix, preferred_element_type=jnp.float32)
    hidden = (jax.nn.silu(gate_act) * up_act).astype(jnp.bfloat16)
    partial_value = jnp.einsum("rf,df->rd", hidden, down_new[0], preferred_element_type=jnp.float32)
    share = lax.psum_scatter(
        partial_value.astype(jnp.bfloat16), "tp", scatter_dimension=1, tiled=True
    )
    back_part = lax.all_to_all(
        share.reshape(fs_count, per_peer, col_count), "fs", split_axis=0, concat_axis=0, tiled=True
    )
    returned = lax.all_gather(back_part, "tp", axis=2, tiled=True).reshape(-1, width)
    picked = returned[dest_flat].reshape(tok_rows, route_ids.shape[1], width).astype(jnp.float32)
    first_weight = jax.nn.sigmoid(route_logits[:, 0] - route_logits[:, 1])
    second_weight = jax.nn.sigmoid(route_logits[:, 1] - route_logits[:, 0])
    mixed = (first_weight[:, None] * picked[:, 0] + second_weight[:, None] * picked[:, 1]).astype(
        jnp.bfloat16
    )
    return (mixed, gate_new, up_new, down_new)


def solution(mesh):
    return jax.shard_map(
        body,
        mesh=mesh,
        in_specs=(
            P("fs", None),
            P("fs", None),
            P("fs", None),
            P("fs"),
            P(None, "fs", "tp"),
            P(None, "fs", "tp"),
            P(None, "fs", "tp"),
        ),
        out_specs=(P("fs", None), P("fs", None, "tp"), P("fs", None, "tp"), P("fs", None, "tp")),
        check_vma=False,
    )
```

profile of v0, /device:TPU:0, one launch (start us, length us, event | category | flops | bytes accessed | tf_op | source)
XLA Modules:
  0.0 482.2 jit_solution(4758031760930865264)
XLA Ops:
  7.2 0.8 copy.14
  8.0 0.1 eq.31
  8.1 0.1 eq.27
  8.3 0.7 broadcast_multiply_fusion
  9.0 0.9 reduce-window.6
  9.8 0.2 slice_reduce_fusion
  10.1 0.1 copy.13
  10.2 0.1 mul.92
  10.4 0.1 fusion.9
  10.5 2.9 scatter_custom_fusion
  13.4 1.3 convert_reduce_fusion
  14.8 1.5 fusion.2
  16.3 1.6 fusion.3
  17.9 0.1 concatenate.3
  18.0 4.2 gather_fusion
  22.2 2.7 constant_dynamic-slice_fusion
  24.9 8.4 %all-to-all-start = ((bf16[16,48,1024]{2,1,0:T(8,128)(2,1)}), bf16[16,48,1024]{2,1,0:T(8,128)(2,1)}, u32[]{:S(2)}, u32[]{:S(2)}) async-start(bf16[16,48,1024]{2,1,0:T(8,128)(2,1)} %constant_dynamic-slice_fusion), calls=%async_computation | async-start | bytes 3145728 | tf_op jit(solution)/shard_map/all_to_all | solution.py:45
  33.3 6.1 %multiply_convert_fusion = (bf16[8,128,1024]{2,1,0:T(8,128)(2,1)S(1)}, bf16[8,128,1024]{2,1,0:T(8,128)(2,1)}) fusion(f32[8,128,1024]{2,1,0:T(8,128)} %param.12, f32[128]{0:T(128)S(1)} %copy-done.2, f32[8,128,1024]{2,1,0:T(8,128)} %param.11), kind=kLoop, calls=%fused_computation.3 | loop fusion | flops 4194304 | bytes 12583424 | tf_op jit(solution)/shard_map/convert_element_type | solution.py:18
  39.4 28.0 %all-to-all-done = bf16[16,48,1024]{2,1,0:T(8,128)(2,1)} async-done(((bf16[16,48,1024]{2,1,0:T(8,128)(2,1)}), bf16[16,48,1024]{2,1,0:T(8,128)(2,1)}, u32[]{:S(2)}, u32[]{:S(2)}) %all-to-all-start) | async-done | bytes 1572896 | tf_op jit(solution)/shard_map/all_to_all | solution.py:45
  67.5 2.1 broadcast_in_dim.12
  69.6 100.9 %all_to_all.46 = bf16[16,128,1024]{2,1,0:T(8,128)(2,1)} all-to-all(bf16[16,128,1024]{2,1,0:T(8,128)(2,1)S(1)} %bitcast.48), channel_id=1, replica_groups=mesh['fs'=16,'tp'=2] {'fs'}, dimensions={0} | all-to-all | bytes 8388608 | tf_op jit(solution)/shard_map/all_to_all | solution.py:21
  170.5 2.6 broadcast_in_dim.13
  173.1 4.5 all-to-all-start.2
  177.6 2.5 convert_element_type.44
  180.2 75.9 %all-to-all-done.2 = bf16[16,128,1024]{2,1,0:T(8,128)(2,1)} async-done(((bf16[16,128,1024]{2,1,0:T(8,128)(2,1)}), bf16[16,128,1024]{2,1,0:T(8,128)(2,1)}, u32[]{:S(2)}, u32[]{:S(2)}) %all-to-all-start.2) | async-done | bytes 4194336 | tf_op jit(solution)/shard_map/all_to_all | solution.py:22
  256.1 2.6 broadcast_in_dim.28
  258.7 18.6 %all-to-all-start.3 = ((bf16[16,128,1024]{2,1,0:T(8,128)(2,1)}), bf16[16,128,1024]{2,1,0:T(8,128)(2,1)}, u32[]{:S(2)}, u32[]{:S(2)}) async-start(bf16[16,128,1024]{2,1,0:T(8,128)(2,1)} %bitcast.46), calls=%async_computation.3 | async-start | bytes 8388608 | tf_op jit(solution)/shard_map/all_to_all | solution.py:23
  277.3 0.0 all-gather.3.cloned.1.call-start
  277.3 0.7 all-gather.3.cloned.1.call-update
  278.0 0.2 reduce-scatter.2.cloned.1.call-start
  278.2 14.8 %all-gather.3.cloned.1.call-done = bf16[768,2048]{1,0:T(8,128)(2,1)} async-done(((bf16[768,1024]{1,0:T(8,128)(2,1)}), bf16[768,2048]{1,0:T(8,128)(2,1)}) %all-gather.3.cloned.1.call-update) | async-done | bytes 3145744 | tf_op jit(solution)/shard_map/all_gather | solution.py:48
  293.0 8.2 %fusion.20 = f32[768,1024]{1,0:T(8,128)} fusion(bf16[768,2048]{1,0:T(8,128)(2,1)} %all-gather.3.cloned.1.call-done, bf16[2048,1024]{1,0:T(8,128)(2,1)} %bitcast.44), kind=kOutput, calls=%fused_computation.54 | convolution fusion | flops 3221225472 | bytes 10485760 | tf_op jit(solution)/shard_map/dot_general | solution.py:49
  301.2 54.5 %all-to-all-done.3 = bf16[16,128,1024]{2,1,0:T(8,128)(2,1)} async-done(((bf16[16,128,1024]{2,1,0:T(8,128)(2,1)}), bf16[16,128,1024]{2,1,0:T(8,128)(2,1)}, u32[]{:S(2)}, u32[]{:S(2)}) %all-to-all-start.3) | async-done | bytes 4194336 | tf_op jit(solution)/shard_map/all_to_all | solution.py:23
  355.7 12.5 %convolution_convert_fusion = bf16[768,2048]{1,0:T(8,128)(2,1)} fusion(bf16[2048,1024]{1,0:T(8,128)(2,1)} %bitcast.10, f32[768,1024]{1,0:T(8,128)} %fusion.20, bf16[768,2048]{1,0:T(8,128)(2,1)} %all-gather.3.cloned.1.call-done, bf16[2048,1024]{1,0:T(8,128)(2,1)} %bitcast.8), kind=kOutput, calls=%fused_computation.5 | convolution fusion | flops 6448742400 | bytes 17825792 | tf_op jit(solution)/shard_map/rf,df->rd/dot_general | solution.py:52
  368.3 0.0 reduce-scatter.2.cloned.1.call-update
  368.3 0.0 copy-start.1
  368.3 0.0 all-gather.5.cloned.1.call-start
  368.4 24.9 %reduce-scatter.2.cloned.1.call-done = bf16[768,1024]{1,0:T(8,128)(2,1)} async-done(((bf16[768,2048]{1,0:T(8,128)(2,1)}), bf16[768,1024]{1,0:T(8,128)(2,1)}) %reduce-scatter.2.cloned.1.call-update) | async-done | bytes 1572880 | tf_op jit(solution)/shard_map/reduce_scatter | solution.py:53
  393.2 44.9 %all_to_all.47 = bf16[16,48,1024]{2,1,0:T(8,128)(2,1)} all-to-all(bf16[16,48,1024]{2,1,0:T(8,128)(2,1)} %bitcast.50), channel_id=1, replica_groups=mesh['fs'=16,'tp'=2] {'fs'}, dimensions={0} | all-to-all | bytes 3145728 | tf_op jit(solution)/shard_map/all_to_all | solution.py:56
  438.1 0.0 all-gather.5.cloned.1.call-update
  438.2 10.6 %all-gather.5.cloned.1.call-done = bf16[16,48,2048]{2,1,0:T(8,128)(2,1)} async-done(((bf16[16,48,1024]{2,1,0:T(8,128)(2,1)}), bf16[16,48,2048]{2,1,0:T(8,128)(2,1)}) %all-gather.5.cloned.1.call-update) | async-done | bytes 3145744 | tf_op jit(solution)/shard_map/all_gather | solution.py:59
  448.7 7.3 %gather_fusion.1 = bf16[384,2048]{1,0:T(8,128)(2,1)} fusion(bf16[768,2048]{1,0:T(8,128)(2,1)} %bitcast.43, s32[1024]{0:T(1024)S(1)} %pad_clamp_fusion), kind=kCustom, calls=%fused_computation.1 | custom fusion | bytes 3147264 | tf_op jit(solution)/shard_map/gather | solution.py:60
  456.1 3.4 reshape.184
  459.5 2.4 fusion.19
  461.9 2.5 fusion.6
  464.4 2.0 copy.35
  466.4 4.6 copy.36
  471.0 4.6 copy.37
  (15 shorter events, 0.1 us)
Async XLA Ops:
  22.2 11.1 %copy-start.2 = (f32[128]{0:T(128)S(1)}, f32[128]{0:T(128)}, u32[]{:S(2)}) copy-start(f32[128]{0:T(128)} %param.10) | copy-start | bytes 1540
  24.9 42.6 %all-to-all-start = ((bf16[16,48,1024]{2,1,0:T(8,128)(2,1)}), bf16[16,48,1024]{2,1,0:T(8,128)(2,1)}, u32[]{:S(2)}, u32[]{:S(2)}) async-start(bf16[16,48,1024]{2,1,0:T(8,128)(2,1)} %constant_dynamic-slice_fusion), calls=%async_computation | async-start | bytes 3145728 | tf_op jit(solution)/shard_map/all_to_all | solution.py:45
  173.1 83.0 %all-to-all-start.2 = ((bf16[16,128,1024]{2,1,0:T(8,128)(2,1)}), bf16[16,128,1024]{2,1,0:T(8,128)(2,1)}, u32[]{:S(2)}, u32[]{:S(2)}) async-start(bf16[16,128,1024]{2,1,0:T(8,128)(2,1)} %bitcast.47), calls=%async_computation.2 | async-start | bytes 8388608 | tf_op jit(solution)/shard_map/all_to_all | solution.py:22
  258.7 97.0 %all-to-all-start.3 = ((bf16[16,128,1024]{2,1,0:T(8,128)(2,1)}), bf16[16,128,1024]{2,1,0:T(8,128)(2,1)}, u32[]{:S(2)}, u32[]{:S(2)}) async-start(bf16[16,128,1024]{2,1,0:T(8,128)(2,1)} %bitcast.46), calls=%async_computation.3 | async-start | bytes 8388608 | tf_op jit(solution)/shard_map/all_to_all | solution.py:23
  277.3 15.7 %all-gather.3.cloned.1.call-start = ((), (), s32[]{:S(2)}) async-start(), calls=%async_computation.6 | async-start | bytes 4718592 | tf_op jit(solution)/shard_map/all_gather | solution.py:48
  278.0 115.2 %reduce-scatter.2.cloned.1.call-start = ((), (), s32[]{:S(2)}) async-start(), calls=%async_computation.7 | async-start | bytes 4718592 | tf_op jit(solution)/shard_map/reduce_scatter | solution.py:53
  368.3 69.8 %copy-start.1 = (f32[192,2]{0,1:T(2,128)S(1)}, f32[192,2]{0,1:T(2,128)}, u32[]{:S(2)}) copy-start(f32[192,2]{0,1:T(2,128)} %param.9) | copy-start | bytes 4612
  368.3 80.4 %all-gather.5.cloned.1.call-start = ((), (), s32[]{:S(2)}) async-start(), calls=%async_computation.8 | async-start | bytes 4718592 | tf_op jit(solution)/shard_map/all_gather | solution.py:59
  459.5 4.9 %copy-start = (bf16[16,128,1024]{2,1,0:T(8,128)(2,1)S(1)}, bf16[16,128,1024]{2,1,0:T(8,128)(2,1)}, u32[]{:S(2)}) copy-start(bf16[16,128,1024]{2,1,0:T(8,128)(2,1)} %all_to_all.46) | copy-start | bytes 12582916
Sparse Core Ops, SparseCore 0:
  279.6 13.3 all-gather.2
  368.4 24.7 reduce-scatter.1
  438.2 10.4 all-gather.4
where the time goes:
time: 483 us; the launch traced here: 482 us
  waiting for transfers between devices  209 us (43%)
  blocking collectives  146 us (30%)
  local copies, waits for them, and re-layouts  43.4 us (9%)
  starting transfers between devices  31.8 us (7%)
  matrix products  20.8 us (4%)
  other arithmetic  17.3 us (4%)
  between operations  13.9 us (3%)
    all_to_all x1, blocking collectives, body(): lax.all_to_all(gate_send, 'fs', split_axis=0, concat_axis=1, tiled=True)  101 us
    all_to_all x1, waiting for transfers between devices, body(): lax.all_to_all(up_send, 'fs', split_axis=0, concat_axis=1, tiled=True)  75.9 us
    all_to_all x1, waiting for transfers between devices, body(): lax.all_to_all(down_send, 'fs', split_axis=0, concat_axis=1, tiled=True)  54.5 us
    all_to_all x1, blocking collectives, body(): lax.all_to_all(share.reshape(fs_count, per_peer, col_count), 'fs', split_...  44.9 us
    all_to_all x1, waiting for transfers between devices, body(): lax.all_to_all(own_cols, 'fs', split_axis=0, concat_axis=0, tiled=True)  28 us
    reduce_scatter x1, waiting for transfers between devices, body(): lax.psum_scatter(partial_value.astype(jnp.bfloat16), 'tp', scatter_dimens...  24.9 us
    all_to_all x1, starting transfers between devices, body(): lax.all_to_all(down_send, 'fs', split_axis=0, concat_axis=1, tiled=True)  18.6 us
    all_gather x1, waiting for transfers between devices, body(): piece = lax.all_gather(arrived, 'tp', axis=1, tiled=True)  14.8 us
  transfers between devices with their start and end apart: 6, of which 6 were waited for; matrix products, arithmetic and copies ran while one was open for 3% of the time, Pallas kernels for 0%

commit v1 on v0

v1 whole, which is shorter than its diff:
```python
import jax
import jax.numpy as jnp
from jax import lax
from jax.sharding import PartitionSpec as P

CAP = 96


def after(value, *earlier):
    return lax.optimization_barrier((value,) + earlier)[0]


def body(tokens, route_ids, route_logits, norm_gain, gate_weight, up_weight, down_weight):
    experts = gate_weight.shape[0]
    fs_count = lax.axis_size("fs")
    tp_count = lax.axis_size("tp")
    copies = fs_count // experts
    width = tokens.shape[1]
    lane = lax.axis_index("fs") % copies
    tp_index = lax.axis_index("tp")
    planes = [[e * copies + c for e in range(experts)] for c in range(copies)]

    def exchange(value):
        return lax.all_to_all(
            value, "fs", split_axis=0, concat_axis=0, tiled=True, axis_index_groups=planes
        )

    def hand_round(value):
        return [
            lax.ppermute(
                value,
                "fs",
                [
                    (e * copies + c, e * copies + (c + step) % copies)
                    for e in range(experts)
                    for c in range(copies)
                ],
            )
            for step in range(1, copies)
        ]

    def weave(own, others):
        if copies == 2:
            parts = [
                jnp.where(lane == 0, own, others[0]),
                jnp.where(lane == 0, others[0], own),
            ]
            joined = jnp.stack(parts, axis=1)
        else:
            held = jnp.stack([own] + others)
            joined = jnp.moveaxis(held[(lane - jnp.arange(copies)) % copies], 0, 1)
        return joined.reshape(1, -1, own.shape[-1])

    def other_core(value):
        return lax.ppermute(value, "tp", [(0, 1), (1, 0)])

    def join_cols(part):
        if tp_count == 2:
            other = other_core(part)
            return jnp.where(
                tp_index == 0,
                jnp.concatenate([part, other], axis=1),
                jnp.concatenate([other, part], axis=1),
            )
        return lax.all_gather(part, "tp", axis=1, tiled=True)

    def sum_cols(partial):
        if tp_count == 2:
            half = partial.shape[1] // 2
            low, high = partial[:, :half], partial[:, half:]
            kept = jnp.where(tp_index == 0, low, high)
            given = jnp.where(tp_index == 0, high, low)
            return (kept.astype(jnp.float32) + other_core(given).astype(jnp.float32)).astype(
                jnp.bfloat16
            )
        return lax.psum_scatter(partial, "tp", scatter_dimension=1, tiled=True)

    scaled_gain = norm_gain[None, :, None]
    gate_own = exchange((scaled_gain * gate_weight).astype(jnp.bfloat16))
    gate_others = hand_round(gate_own)

    values = tokens.astype(jnp.float32)
    center = jnp.mean(values, axis=1, keepdims=True)
    spread = jnp.mean(jnp.square(values - center), axis=1, keepdims=True)
    normed = ((values - center) * lax.rsqrt(spread + 1e-06)).astype(jnp.bfloat16)
    rows = tokens.shape[0]
    names = jnp.arange(experts, dtype=jnp.int32)
    named = jnp.any(route_ids[:, :, None] == names[None, None, :], axis=1)
    row_no = jnp.arange(rows, dtype=jnp.int32)
    earlier = (row_no[:, None] > row_no[None, :]).astype(jnp.bfloat16)
    before = jnp.dot(earlier, named.astype(jnp.bfloat16), preferred_element_type=jnp.float32)
    place = jnp.where(named, before.astype(jnp.int32), CAP)
    slots = jnp.arange(CAP, dtype=jnp.int32)
    pick = (place.T[:, None, :] == slots[None, :, None]).astype(jnp.bfloat16)
    pick = pick.reshape(experts * CAP, rows)
    col_count = width // tp_count
    own_cols = lax.dynamic_slice_in_dim(normed, tp_index * col_count, col_count, 1)
    send_rows = jnp.dot(pick, own_cols, preferred_element_type=jnp.float32).astype(jnp.bfloat16)

    up_send = (scaled_gain * up_weight).astype(jnp.bfloat16)
    up_own = exchange(after(up_send, gate_own))
    up_others = hand_round(up_own)
    arrived = exchange(after(send_rows.reshape(experts, CAP, col_count), up_own, gate_others[0]))
    piece = join_cols(arrived.reshape(-1, col_count))
    down_send = down_weight.astype(jnp.bfloat16)
    down_own = exchange(after(down_send, arrived, up_others[0]))
    down_others = hand_round(down_own)

    gate_new = weave(gate_own, gate_others)
    up_new = weave(up_own, up_others)
    down_new = weave(down_own, down_others)

    gate_act = jnp.dot(piece, gate_new[0], preferred_element_type=jnp.float32)
    up_act = jnp.dot(piece, up_new[0], preferred_element_type=jnp.float32)
    hidden = (jax.nn.silu(gate_act) * up_act).astype(jnp.bfloat16)
    partial_value = jnp.einsum(
        "rf,df->rd", hidden, down_new[0], preferred_element_type=jnp.float32
    ).astype(jnp.bfloat16)
    share = sum_cols(partial_value)
    returned = exchange(share.reshape(experts, CAP, col_count)).reshape(experts * CAP, col_count)

    def chosen(k):
        spot = jnp.sum(
            jnp.where(route_ids[:, k, None] == names[None, :], place + CAP * names[None, :], 0),
            axis=1,
        )
        hot = (spot[:, None] == jnp.arange(experts * CAP, dtype=jnp.int32)[None, :]).astype(
            jnp.bfloat16
        )
        return jnp.dot(hot, returned, preferred_element_type=jnp.float32)

    first_weight = jax.nn.sigmoid(route_logits[:, 0] - route_logits[:, 1])
    second_weight = jax.nn.sigmoid(route_logits[:, 1] - route_logits[:, 0])
    mixed_cols = (
        first_weight[:, None] * chosen(0) + second_weight[:, None] * chosen(1)
    ).astype(jnp.bfloat16)
    mixed = join_cols(mixed_cols)
    return (mixed, gate_new, up_new, down_new)


def solution(mesh):
    return jax.shard_map(
        body,
        mesh=mesh,
        in_specs=(
            P("fs", None),
            P("fs", None),
            P("fs", None),
            P("fs"),
            P(None, "fs", "tp"),
            P(None, "fs", "tp"),
            P(None, "fs", "tp"),
        ),
        out_specs=(P("fs", None), P("fs", None, "tp"), P("fs", None, "tp"), P("fs", None, "tp")),
        check_vma=False,
    )
```

time: 483 us -> 342 us (0.71)
  waiting for transfers between devices: 209 us -> 166 us
  local copies, waits for them, and re-layouts: 43.4 us -> 3.16 us
  blocking collectives: 146 us -> 107 us
  starting transfers between devices: 31.8 us -> 17.8 us
  between operations: 13.9 us -> 0.8 us
  other arithmetic: 17.3 us -> 23 us
    ppermute x0 -> x6, waiting for transfers between devices: none -> 128 us  [the longest x3 123 us: hand_round(): lax.ppermute(value, 'fs', [(e * copies + c, e * copies + (c + step) % cop...]
    all_to_all x3, waiting for transfers between devices: 158 us -> 38.1 us  [exchange(): lax.all_to_all(value, 'fs', split_axis=0, concat_axis=0, tiled=True, axis...]
    all_to_all x2, blocking collectives: 146 us -> 107 us  [exchange(): lax.all_to_all(value, 'fs', split_axis=0, concat_axis=0, tiled=True, axis...]
    all_gather x2 -> x0, waiting for transfers between devices: 25.3 us -> none  [the longest x1 14.8 us: body(): piece = lax.all_gather(arrived, 'tp', axis=1, tiled=True)]
    reduce_scatter x1 -> x0, waiting for transfers between devices: 24.9 us -> none  [body(): lax.psum_scatter(partial_value.astype(jnp.bfloat16), 'tp', scatter_dimens...]
    all_to_all x3, starting transfers between devices: 31.5 us -> 13.1 us  [exchange(): lax.all_to_all(value, 'fs', split_axis=0, concat_axis=0, tiled=True, axis...]
    unnamed x10, local copies, waits for them, and re-layouts: 12.1 us -> 0.02 us
    gather x2 -> x0, local copies, waits for them, and re-layouts: 11.6 us -> none  [the longest x1 7.34 us: body(): returned[dest_flat].reshape(tok_rows, route_ids.shape[1], width)]
  transfers between devices with their start and end apart: 6 -> 9, of which waited for: 6 -> 7; matrix products, arithmetic and copies ran while one was open for 3% -> 5% of each run, Pallas kernels for 0% -> 0%
where the time goes in v1:
time: 342 us
  waiting for transfers between devices  166 us (49%)
  blocking collectives  107 us (31%)
  matrix products  24 us (7%)
  other arithmetic  23 us (7%)
  starting transfers between devices  17.8 us (5%)
    ppermute x3, waiting for transfers between devices, hand_round(): lax.ppermute(value, 'fs', [(e * copies + c, e * copies + (c + step) % cop...  123 us
    all_to_all x2, blocking collectives, exchange(): lax.all_to_all(value, 'fs', split_axis=0, concat_axis=0, tiled=True, axis...  107 us
    all_to_all x3, waiting for transfers between devices, exchange(): lax.all_to_all(value, 'fs', split_axis=0, concat_axis=0, tiled=True, axis...  38.1 us
    all_to_all x3, starting transfers between devices, exchange(): lax.all_to_all(value, 'fs', split_axis=0, concat_axis=0, tiled=True, axis...  13.1 us
    dot_general x1, matrix products, body(): jnp.einsum('rf,df->rd', hidden, down_new[0], preferred_element_type=jnp.f...  12 us
    dot_general x1, matrix products, body(): up_act = jnp.dot(piece, up_new[0], preferred_element_type=jnp.float32)  8.98 us
    another operation x5, other arithmetic, weave(): joined = jnp.stack(parts, axis=1)  8.73 us
  transfers between devices with their start and end apart: 9, of which 7 were waited for; matrix products, arithmetic and copies ran while one was open for 5% of the time, Pallas kernels for 0%

profile of v1, /device:TPU:0, one launch (start us, length us, event | category | flops | bytes accessed | tf_op | source)
XLA Modules:
  0.0 341.9 jit_solution(7081014429539097018)
XLA Ops:
  0.6 6.1 %multiply_convert_fusion = (bf16[8,128,1024]{2,1,0:T(8,128)(2,1)S(1)}, bf16[8,128,1024]{2,1,0:T(8,128)(2,1)}) fusion(f32[8,128,1024]{2,1,0:T(8,128)} %param.11, f32[128]{0:T(128)} %param.10, f32[8,128,1024]{2,1,0:T(8,128)} %param.12), kind=kLoop, calls=%fused_computation.3 | loop fusion | flops 4194304 | bytes 12583424 | tf_op jit(solution)/shard_map/convert_element_type | solution.py:79
  6.8 55.4 %all_to_all.25 = bf16[8,128,1024]{2,1,0:T(8,128)(2,1)} all-to-all(bf16[8,128,1024]{2,1,0:T(8,128)(2,1)S(1)} %get-tuple-element.24), channel_id=1, replica_groups={{0,4,8,12,16,20,24,28},{2,6,10,14,18,22,26,30},{1,5,9,13,17,21,25,29},{..., dimensions={0} | all-to-all | bytes 4194304 | tf_op jit(solution)/shard_map/all_to_all | solution.py:24
  62.2 3.7 %all-to-all-start.1 = ((bf16[8,128,1024]{2,1,0:T(8,128)(2,1)}), bf16[8,128,1024]{2,1,0:T(8,128)(2,1)S(1)}, u32[]{:S(2)}, u32[]{:S(2)}) async-start(bf16[8,128,1024]{2,1,0:T(8,128)(2,1)} %get-tuple-element.7), calls=%async_computation.1 | async-start | bytes 4194304 | tf_op jit(solution)/shard_map/all_to_all | solution.py:24
  65.9 1.6 collective-permute-start
  67.5 0.1 eq.119
  67.6 0.0 copy-done.2
  67.6 0.2 select_reduce_fusion
  67.8 0.2 bitcast_compare_fusion
  68.0 0.0 copy-done.1
  68.0 0.2 convert_reduce_fusion
  68.2 0.4 multiply_reduce_fusion
  68.6 1.8 convolution_convert_fusion.1
  70.4 42.6 %collective-permute-done = bf16[8,128,1024]{2,1,0:T(8,128)(2,1)} collective-permute-done((bf16[8,128,1024]{2,1,0:T(8,128)(2,1)}, bf16[8,128,1024]{2,1,0:T(8,128)(2,1)}, u32[]{:S(2)}, u32[]{:S(2)}) %collective-permute-start) | collective-permute-done | bytes 2097184 | tf_op jit(solution)/shard_map/ppermute | solution.py:30
  113.0 0.8 all-to-all-done.1
  113.8 4.9 %all-to-all-start.2 = ((bf16[8,96,1024]{2,1,0:T(8,128)(2,1)}), bf16[8,96,1024]{2,1,0:T(8,128)(2,1)}, u32[]{:S(2)}, u32[]{:S(2)}) async-start(bf16[8,96,1024]{2,1,0:T(8,128)(2,1)} %bitcast.40), calls=%async_computation.2 | async-start | bytes 3145728 | tf_op jit(solution)/shard_map/all_to_all | solution.py:24
  118.7 1.5 collective-permute-start.2
  120.2 3.8 %convert_element_type.53 = bf16[8,128,1024]{2,1,0:T(8,128)(2,1)} convert(f32[8,128,1024]{2,1,0:T(8,128)} %param.13) | non-fusion elementwise | flops 1048576 | bytes 6291456 | tf_op jit(solution)/shard_map/convert_element_type | solution.py:105
  124.0 40.8 %collective-permute-done.2 = bf16[8,128,1024]{2,1,0:T(8,128)(2,1)} collective-permute-done((bf16[8,128,1024]{2,1,0:T(8,128)(2,1)S(1)}, bf16[8,128,1024]{2,1,0:T(8,128)(2,1)}, u32[]{:S(2)}, u32[]{:S(2)}) %collective-permute-start.2) | collective-permute-done | bytes 2097184 | tf_op jit(solution)/shard_map/ppermute | solution.py:30
  164.8 0.0 all-to-all-done.2
  164.8 51.6 %all_to_all.26 = bf16[8,128,1024]{2,1,0:T(8,128)(2,1)} all-to-all(bf16[8,128,1024]{2,1,0:T(8,128)(2,1)} %convert_element_type.53), channel_id=1, replica_groups={{0,4,8,12,16,20,24,28},{2,6,10,14,18,22,26,30},{1,5,9,13,17,21,25,29},{..., dimensions={0} | all-to-all | bytes 4194304 | tf_op jit(solution)/shard_map/all_to_all | solution.py:24
  216.4 1.5 collective-permute-start.3
  217.9 0.0 collective-permute-start.1
  217.9 2.5 select_bitcast_fusion.5
  220.4 2.4 pad_maximum_fusion
  222.8 39.5 %collective-permute-done.3 = bf16[8,128,1024]{2,1,0:T(8,128)(2,1)} collective-permute-done((bf16[8,128,1024]{2,1,0:T(8,128)(2,1)}, bf16[8,128,1024]{2,1,0:T(8,128)(2,1)}, u32[]{:S(2)}, u32[]{:S(2)}) %collective-permute-start.3) | collective-permute-done | bytes 2097184 | tf_op jit(solution)/shard_map/ppermute | solution.py:30
  262.3 3.1 select_bitcast_fusion.1
  265.4 0.4 pad_maximum_fusion.2
  265.8 2.5 copy.27
  268.2 0.4 pad_maximum_fusion.1
  268.6 0.6 copy.26
  269.2 0.0 copy-start
  269.2 0.0 collective-permute-done.1
  269.2 0.0 copy-start.4
  269.2 9.0 %fusion.5 = f32[768,1024]{1,0:T(8,128)} fusion(bf16[2048,1024]{1,0:T(8,128)(2,1)S(1)} %bitcast.46, bf16[768,1024]{1,0:T(8,128)(2,1)S(1)} %collective-permute-done.1, bf16[768,1024]{1,0:T(8,128)(2,1)} %bitcast.5, pred[]{:T(512)S(6)} %eq.53), kind=kOutput, calls=%fused_computation.33 | convolution fusion | flops 3235381248 | bytes 10485761 | tf_op jit(solution)/shard_map/dot_general | solution.py:114
  278.2 0.0 copy-done.4
  278.2 12.0 %convolution_convert_fusion = bf16[768,2048]{1,0:T(8,128)(2,1)S(1)} fusion(bf16[2048,1024]{1,0:T(8,128)(2,1)} %bitcast.44, f32[768,1024]{1,0:T(8,128)} %fusion.5, bf16[2048,1024]{1,0:T(8,128)(2,1)} %bitcast.42, bf16[768,1024]{1,0:T(8,128)(2,1)} %copy-done.4, bf16[768,1024]{1,0:T(8,128)(2,1)} %bitcast.5, pred[]{:T(512)S(6)} %eq.53), kind=kOutput, calls=%fused_computation.5 | convolution fusion | flops 6462898176 | bytes 17825792 | tf_op jit(solution)/shard_map/rf,df->rd/dot_general | solution.py:116
  290.2 0.2 broadcast_select_fusion
  290.4 0.1 collective-permute-start.4
  290.4 3.4 collective-permute-done.4
  293.8 2.2 add_convert_fusion
  296.0 4.5 %all-to-all-start.4 = ((bf16[8,96,1024]{2,1,0:T(8,128)(2,1)}), bf16[8,96,1024]{2,1,0:T(8,128)(2,1)S(1)}, u32[]{:S(2)}, u32[]{:S(2)}) async-start(bf16[8,96,1024]{2,1,0:T(8,128)(2,1)} %bitcast.41), calls=%async_computation.4 | async-start | bytes 3145728 | tf_op jit(solution)/shard_map/all_to_all | solution.py:24
  300.5 0.0 copy-done.3
  300.6 37.3 %all-to-all-done.4 = bf16[8,96,1024]{2,1,0:T(8,128)(2,1)S(1)} async-done(((bf16[8,96,1024]{2,1,0:T(8,128)(2,1)}), bf16[8,96,1024]{2,1,0:T(8,128)(2,1)S(1)}, u32[]{:S(2)}, u32[]{:S(2)}) %all-to-all-start.4) | async-done | bytes 1572896 | tf_op jit(solution)/shard_map/all_to_all | solution.py:24
  337.9 0.5 convolution_multiply_fusion.1
  338.4 0.5 fusion.2
  338.9 0.1 collective-permute-start.5
  339.0 1.7 collective-permute-done.5
  340.7 1.2 maximum_select_fusion.1
  (11 shorter events, 0.1 us)
Async XLA Ops:
  62.2 5.4 %copy-start.2 = (s32[192,2]{0,1:T(2,128)S(1)}, s32[192,2]{0,1:T(2,128)}, u32[]{:S(2)}) copy-start(s32[192,2]{0,1:T(2,128)} %param.8) | copy-start | bytes 4612
  62.2 5.8 %copy-start.1 = (bf16[192,2048]{1,0:T(8,128)(2,1)S(1)}, bf16[192,2048]{1,0:T(8,128)(2,1)}, u32[]{:S(2)}) copy-start(bf16[192,2048]{1,0:T(8,128)(2,1)} %param.7) | copy-start | bytes 2359300
  62.2 51.6 %all-to-all-start.1 = ((bf16[8,128,1024]{2,1,0:T(8,128)(2,1)}), bf16[8,128,1024]{2,1,0:T(8,128)(2,1)S(1)}, u32[]{:S(2)}, u32[]{:S(2)}) async-start(bf16[8,128,1024]{2,1,0:T(8,128)(2,1)} %get-tuple-element.7), calls=%async_computation.1 | async-start | bytes 4194304 | tf_op jit(solution)/shard_map/all_to_all | solution.py:24
  65.9 47.0 %collective-permute-start = (bf16[8,128,1024]{2,1,0:T(8,128)(2,1)}, bf16[8,128,1024]{2,1,0:T(8,128)(2,1)}, u32[]{:S(2)}, u32[]{:S(2)}) collective-permute-start(bf16[8,128,1024]{2,1,0:T(8,128)(2,1)} %all_to_all.25), channel_id=1, source_target_pairs={{0,2},{2,0},{4,6},{6,4},{8,10},{10,8},{12,14},{14,12},{16,18},{18,... | collective-permute-start | bytes 6291464 | tf_op jit(solution)/shard_map/ppermute | solution.py:30
  113.8 51.0 %all-to-all-start.2 = ((bf16[8,96,1024]{2,1,0:T(8,128)(2,1)}), bf16[8,96,1024]{2,1,0:T(8,128)(2,1)}, u32[]{:S(2)}, u32[]{:S(2)}) async-start(bf16[8,96,1024]{2,1,0:T(8,128)(2,1)} %bitcast.40), calls=%async_computation.2 | async-start | bytes 3145728 | tf_op jit(solution)/shard_map/all_to_all | solution.py:24
  118.7 46.1 %collective-permute-start.2 = (bf16[8,128,1024]{2,1,0:T(8,128)(2,1)S(1)}, bf16[8,128,1024]{2,1,0:T(8,128)(2,1)}, u32[]{:S(2)}, u32[]{:S(2)}) collective-permute-start(bf16[8,128,1024]{2,1,0:T(8,128)(2,1)S(1)} %all-to-all-done.1), channel_id=1, source_target_pairs={{0,2},{2,0},{4,6},{6,4},{8,10},{10,8},{12,14},{14,12},{16,18},{18,... | collective-permute-start | bytes 6291464 | tf_op jit(solution)/shard_map/ppermute | solution.py:30
  216.4 45.9 %collective-permute-start.3 = (bf16[8,128,1024]{2,1,0:T(8,128)(2,1)}, bf16[8,128,1024]{2,1,0:T(8,128)(2,1)}, u32[]{:S(2)}, u32[]{:S(2)}) collective-permute-start(bf16[8,128,1024]{2,1,0:T(8,128)(2,1)} %all_to_all.26), channel_id=1, source_target_pairs={{0,2},{2,0},{4,6},{6,4},{8,10},{10,8},{12,14},{14,12},{16,18},{18,... | collective-permute-start | bytes 6291464 | tf_op jit(solution)/shard_map/ppermute | solution.py:30
  217.9 51.3 %collective-permute-start.1 = (bf16[768,1024]{1,0:T(8,128)(2,1)}, bf16[768,1024]{1,0:T(8,128)(2,1)S(1)}, u32[]{:S(2)}, u32[]{:S(2)}) collective-permute-start(bf16[768,1024]{1,0:T(8,128)(2,1)} %bitcast.5), channel_id=1, source_target_pairs={{0,1},{1,0},{2,3},{3,2},{4,5},{5,4},{6,7},{7,6},{8,9},{9,8},{10,11... | collective-permute-start | bytes 4718600 | tf_op jit(solution)/shard_map/ppermute | solution.py:55
  269.2 9.0 %copy-start = (bf16[8,2,128,1024]{3,2,1,0:T(8,128)(2,1)}, bf16[8,2,128,1024]{3,2,1,0:T(8,128)(2,1)S(1)}, u32[]{:S(2)}) copy-start(bf16[8,2,128,1024]{3,2,1,0:T(8,128)(2,1)S(1)} %copy.26) | copy-start | bytes 12582916
  269.2 9.0 %copy-start.4 = (bf16[768,1024]{1,0:T(8,128)(2,1)}, bf16[768,1024]{1,0:T(8,128)(2,1)S(1)}, u32[]{:S(2)}) copy-start(bf16[768,1024]{1,0:T(8,128)(2,1)S(1)} %collective-permute-done.1) | copy-start | bytes 4718596
  290.4 3.5 %collective-permute-start.4 = (bf16[768,1024]{1,0:T(8,128)(2,1)S(1)}, bf16[768,1024]{1,0:T(8,128)(2,1)S(1)}, u32[]{:S(2)}, u32[]{:S(2)}) collective-permute-start(bf16[768,1024]{1,0:T(8,128)(2,1)S(1)} %broadcast_select_fusion), channel_id=1, source_target_pairs={{0,1},{1,0},{2,3},{3,2},{4,5},{5,4},{6,7},{7,6},{8,9},{9,8},{10,11... | collective-permute-start | bytes 4718600 | tf_op jit(solution)/shard_map/ppermute | solution.py:55
  296.0 4.5 %copy-start.3 = (f32[192,2]{0,1:T(2,128)S(1)}, f32[192,2]{0,1:T(2,128)}, u32[]{:S(2)}) copy-start(f32[192,2]{0,1:T(2,128)} %param.9) | copy-start | bytes 4612
  296.0 41.8 %all-to-all-start.4 = ((bf16[8,96,1024]{2,1,0:T(8,128)(2,1)}), bf16[8,96,1024]{2,1,0:T(8,128)(2,1)S(1)}, u32[]{:S(2)}, u32[]{:S(2)}) async-start(bf16[8,96,1024]{2,1,0:T(8,128)(2,1)} %bitcast.41), calls=%async_computation.4 | async-start | bytes 3145728 | tf_op jit(solution)/shard_map/all_to_all | solution.py:24
  338.9 1.8 collective-permute-start.5

commit v2 on v1

v2 whole, which is shorter than its diff:
```python
import functools

import jax
import jax.numpy as jnp
import numpy as np
from jax import lax
from jax.experimental import pallas as pl
from jax.experimental.pallas import tpu as pltpu
from jax.sharding import PartitionSpec as P

CAP = 96


def after(value, *earlier):
    return lax.optimization_barrier((value,) + earlier)[0]


def place_kernel(moves, number, where_ref, *refs):
    arrays, outs = refs[:number], refs[number : -2 - number]
    held = refs[-2 - number : -2]
    in_sems, out_sems = refs[-2:]
    loads = [
        pltpu.make_async_copy(array, held[i], in_sems.at[i]) for i, array in enumerate(arrays)
    ]
    for load in loads:
        load.start()
    stores = []
    seen = set()
    for n, (i, part, first, rows, out, start, slot) in enumerate(moves):
        if i not in seen:
            loads[i].wait()
            seen.add(i)
        store = pltpu.make_async_copy(
            held[i].at[part, pl.ds(first, rows)],
            outs[out].at[where_ref[slot], pl.ds(start, rows)],
            out_sems.at[n],
        )
        store.start()
        stores.append(store)
    for store in stores:
        store.wait()


def place(arrays, moves, where, out_shapes):
    dtype = arrays[0].dtype
    hbm = pl.BlockSpec(memory_space=pltpu.HBM)
    size = 2 * sum(int(np.prod(a.shape)) for a in arrays)
    return pl.pallas_call(
        functools.partial(place_kernel, moves, len(arrays)),
        grid_spec=pltpu.PrefetchScalarGridSpec(
            num_scalar_prefetch=1,
            grid=(),
            in_specs=[hbm] * len(arrays),
            out_specs=[hbm] * len(out_shapes),
            scratch_shapes=[pltpu.VMEM(a.shape, dtype) for a in arrays]
            + [
                pltpu.SemaphoreType.DMA((len(arrays),)),
                pltpu.SemaphoreType.DMA((len(moves),)),
            ],
        ),
        out_shape=[jax.ShapeDtypeStruct(s, dtype) for s in out_shapes],
        cost_estimate=pl.CostEstimate(flops=4 * size, bytes_accessed=2 * size, transcendentals=0),
    )(where, *arrays)


def pick_kernel(layout, cols, where_ref, *refs):
    arrays, out_ref = refs[:-1], refs[-1]
    expert = where_ref[len(layout)]
    slots = lax.broadcasted_iota(jnp.int32, (1, CAP), 1).astype(jnp.float32)
    for n, (i, part) in enumerate(layout):
        block = arrays[i][part]
        extra = block[:, cols:].astype(jnp.float32)
        column = lax.broadcasted_iota(jnp.int32, extra.shape, 1)
        rank = jnp.sum(jnp.where(column == expert, extra, 0.0), axis=1, keepdims=True)
        hot = (rank == slots).astype(jnp.float32).astype(block.dtype)
        rows = lax.dot_general(
            hot, block[:, :cols], (((0,), (0,)), ((), ())), preferred_element_type=jnp.float32
        )
        out_ref[where_ref[n]] = rows.astype(out_ref.dtype)


def pick_rows(arrays, layout, where, cols):
    size = 2 * sum(int(np.prod(a.shape)) for a in arrays)
    rows = arrays[0].shape[1]
    vmem = pl.BlockSpec(memory_space=pltpu.VMEM)
    return pl.pallas_call(
        functools.partial(pick_kernel, layout, cols),
        grid_spec=pltpu.PrefetchScalarGridSpec(
            num_scalar_prefetch=1, grid=(), in_specs=[vmem] * len(arrays), out_specs=vmem
        ),
        out_shape=jax.ShapeDtypeStruct((len(layout), CAP, cols), arrays[0].dtype),
        cost_estimate=pl.CostEstimate(
            flops=2 * len(layout) * CAP * rows * cols, bytes_accessed=2 * size, transcendentals=0
        ),
    )(where, *arrays)


def body(tokens, route_ids, route_logits, norm_gain, gate_weight, up_weight, down_weight):
    experts, depth, cols = gate_weight.shape
    fs_count = lax.axis_size("fs")
    tp_count = lax.axis_size("tp")
    copies = fs_count // experts
    rows, width = tokens.shape
    share_width = width // tp_count
    lane = lax.axis_index("fs") % copies
    expert = lax.axis_index("fs") // copies
    tp_index = lax.axis_index("tp")
    planes = [[e * copies + c for e in range(experts)] for c in range(copies)]

    def exchange(value):
        return lax.all_to_all(
            value, "fs", split_axis=0, concat_axis=0, tiled=True, axis_index_groups=planes
        )

    def hand_round(value):
        return [
            lax.ppermute(
                value,
                "fs",
                [
                    (e * copies + c, e * copies + (c + step) % copies)
                    for e in range(experts)
                    for c in range(copies)
                ],
            )
            for step in range(1, copies)
        ]

    def other_core(value):
        return lax.ppermute(value, "tp", [(0, 1), (1, 0)])

    def join_cols(part):
        if tp_count == 2:
            other = other_core(part)
            return jnp.where(
                tp_index == 0,
                jnp.concatenate([part, other], axis=1),
                jnp.concatenate([other, part], axis=1),
            )
        return lax.all_gather(part, "tp", axis=1, tiled=True)

    cuts = [2 * depth * k // 16 // 16 * 16 for k in (0, 4, 11, 16)]
    spans = list(zip(cuts[:-1], cuts[1:]))
    sources = [gate_weight, up_weight]

    def segments(start, stop):
        found = []
        for n in range(2):
            lo, hi = max(start, n * depth), min(stop, (n + 1) * depth)
            if lo < hi:
                found.append((n, lo - n * depth, hi - lo))
        return found

    def fold(span, *earlier):
        gain = after(norm_gain, *earlier) if earlier else norm_gain
        parts = [
            (gain[None, a : a + size, None] * sources[n][:, a : a + size]).astype(jnp.bfloat16)
            for n, a, size in segments(*span)
        ]
        return jnp.concatenate(parts, axis=1) if len(parts) > 1 else parts[0]

    first_block = fold(spans[0])
    tokens, route_ids = lax.optimization_barrier((tokens, route_ids, first_block))[:2]
    names = jnp.arange(experts, dtype=jnp.int32)
    named = jnp.any(route_ids[:, :, None] == names[None, None, :], axis=1)
    row_no = jnp.arange(rows, dtype=jnp.int32)
    earlier = (row_no[:, None] > row_no[None, :]).astype(jnp.bfloat16)
    before = jnp.dot(earlier, named.astype(jnp.bfloat16), preferred_element_type=jnp.float32)
    rank = jnp.where(named, before.astype(jnp.int32), CAP)
    values = tokens.astype(jnp.float32)
    center = jnp.mean(values, axis=1, keepdims=True)
    spread = jnp.mean(jnp.square(values - center), axis=1, keepdims=True)
    normed = ((values - center) * lax.rsqrt(spread + 1e-06)).astype(jnp.bfloat16)
    own_cols = lax.dynamic_slice_in_dim(normed, tp_index * share_width, share_width, 1)
    extra = jnp.pad(rank.astype(jnp.bfloat16), ((0, 0), (0, 128 - experts)))
    chunk = jnp.concatenate([own_cols, extra], axis=1)

    inner = 2 if copies == 2 else 1
    line = experts // inner
    spot_z = expert // inner
    spot_y = expert % inner

    def along_line(value, step):
        return lax.ppermute(
            value,
            "fs",
            [
                ((z * inner + y) * copies + c, ((z + step) * inner + y) * copies + c)
                for z in range(line)
                if 0 <= z + step < line
                for y in range(inner)
                for c in range(copies)
            ],
        )

    def across(value):
        return lax.ppermute(
            value,
            "fs",
            [
                ((z * inner + y) * copies + c, (z * inner + 1 - y) * copies + c)
                for z in range(line)
                for y in range(inner)
                for c in range(copies)
            ],
        )

    rising = [chunk]
    falling = [chunk]
    for _ in range(1, line):
        rising.append(along_line(rising[-1], 1))
        falling.append(along_line(falling[-1], -1))

    def near(k):
        return jnp.where(spot_z >= k, rising[k], falling[line - k])

    middle = line // 2
    ends = [k for k in range(1, line) if k != middle]
    near_middle = near(middle)
    near_ends = jnp.stack([near(k) for k in ends])
    arrays = [chunk[None], near_middle[None], near_ends]
    if inner == 2:
        far_own = across(chunk)
        far_middle = across(near_middle)
        far_ends = across(near_ends)
        arrays += [far_own[None], far_middle[None], far_ends]
    layout = []
    order = []
    for g in range(inner):
        for k in range(line):
            at = 0 if k == 0 else 1 if k == middle else 2
            layout.append((3 * g + at, ends.index(k) if at == 2 else 0))
            order.append((spot_z - k) % line * inner + (spot_y if g == 0 else 1 - spot_y))
    where = jnp.stack(order + [expert]).astype(jnp.int32)
    piece_cols = pick_rows(arrays, layout, where, share_width)
    piece_cols = piece_cols.reshape(experts * CAP, share_width)
    piece = join_cols(piece_cols)

    spots = jnp.stack(
        [e * copies + (lane - c) % copies for c in range(copies) for e in range(experts)]
    ).astype(jnp.int32)
    shape = (fs_count, depth, cols)
    held = []
    for n, span in enumerate(spans):
        block = first_block if n == 0 else fold(span, chunk)
        if n:
            block = after(block, held[-1][0])
        own = exchange(block)
        held.append([own] + hand_round(own))
    made = []
    for target in range(2):
        parts = []
        moves = []
        for n, span in enumerate(spans):
            first = 0
            for tensor, start, size in segments(*span):
                if tensor == target:
                    moves += [
                        (len(parts) + c, e, first, size, 0, start, c * experts + e)
                        for c in range(copies)
                        for e in range(experts)
                    ]
                    parts += held[n]
                first += size
        made += place(parts, moves, spots, [shape])
    gate_new, up_new = (m.reshape(1, width, cols) for m in made)

    gate_act = jnp.dot(piece, gate_new[0], preferred_element_type=jnp.float32)
    up_act = jnp.dot(piece, up_new[0], preferred_element_type=jnp.float32)
    hidden = (jax.nn.silu(gate_act) * up_act).astype(jnp.bfloat16)
    hidden = after(hidden)

    cuts = [depth * k // 8 for k in (0, 4, 8)]
    spans = list(zip(cuts[:-1], cuts[1:]))
    groups = []
    for n, (start, stop) in enumerate(spans):
        send = after(down_weight[:, start:stop].astype(jnp.bfloat16), chunk)
        send = after(send, groups[-1][0] if n else held[-1][0])
        own = exchange(send)
        groups.append([own] + hand_round(own))
    moves = [
        (g * copies + c, e, 0, stop - start, 0, start, c * experts + e)
        for g, (start, stop) in enumerate(spans)
        for c in range(copies)
        for e in range(experts)
    ]
    (down_new,) = place([a for group in groups for a in group], moves, spots, [shape])
    down_new = down_new.reshape(1, width, cols)

    tenth = experts // tp_count

    def project(group):
        def part(index):
            matrix = jnp.concatenate(
                [lax.dynamic_slice_in_dim(a, index * tenth, tenth, 0) for a in group], axis=0
            ).reshape(-1, cols)
            return jnp.einsum(
                "rf,df->rd", hidden, matrix, preferred_element_type=jnp.float32
            ).astype(jnp.bfloat16)

        if tp_count == 2:
            given = part(1 - tp_index)
            came = other_core(given)
            kept = after(part(tp_index), given)
            share = (kept.astype(jnp.float32) + came.astype(jnp.float32)).astype(
                jnp.bfloat16
            )
        else:
            partial = jnp.concatenate([part(t) for t in range(tp_count)], axis=1)
            share = lax.psum_scatter(partial, "tp", scatter_dimension=1, tiled=True)
        return share.reshape(experts, CAP, -1)

    backs = []
    shares = [hidden]
    for n, group in enumerate(groups):
        group = [after(a, shares[-1]) for a in group]
        shares.append(project(group))
        share = after(shares[-1], backs[-1] if n else groups[-1][0])
        backs.append(exchange(share))

    def hot_rows(k):
        spot = jnp.sum(
            jnp.where(route_ids[:, k, None] == names[None, :], rank + CAP * names[None, :], 0),
            axis=1,
        )
        return (spot[:, None] == jnp.arange(experts * CAP, dtype=jnp.int32)[None, :]).astype(
            jnp.bfloat16
        )

    hot = [hot_rows(0), hot_rows(1)]
    first_weight = jax.nn.sigmoid(route_logits[:, 0] - route_logits[:, 1])[:, None]
    second_weight = jax.nn.sigmoid(route_logits[:, 1] - route_logits[:, 0])[:, None]

    def mix(back):
        back = back.reshape(experts * CAP, -1)
        first, second = (jnp.dot(h, back, preferred_element_type=jnp.float32) for h in hot)
        return (first_weight * first + second_weight * second).astype(jnp.bfloat16)

    order = jnp.concatenate(
        [
            (
                (
                    (jnp.arange(tenth)[None, :, None] * copies)
                    + (lane - jnp.arange(copies)[:, None, None]) % copies
                )
                * depth
                + start
                + jnp.arange(stop - start)[None, None, :]
            ).reshape(-1)
            for start, stop in spans
        ]
    )
    in_order = (order[:, None] == jnp.arange(share_width)[None, :]).astype(jnp.bfloat16)
    mixed_cols = jnp.concatenate([mix(back) for back in backs], axis=1)
    mixed_cols = jnp.dot(mixed_cols, in_order, preferred_element_type=jnp.float32)
    mixed = join_cols(mixed_cols.astype(jnp.bfloat16))
    return (mixed, gate_new, up_new, down_new)


def solution(mesh):
    return jax.shard_map(
        body,
        mesh=mesh,
        in_specs=(
            P("fs", None),
            P("fs", None),
            P("fs", None),
            P("fs"),
            P(None, "fs", "tp"),
            P(None, "fs", "tp"),
            P(None, "fs", "tp"),
        ),
        out_specs=(P("fs", None), P("fs", None, "tp"), P("fs", None, "tp"), P("fs", None, "tp")),
        check_vma=False,
    )
```

time: 342 us -> 332 us (0.971)
  blocking collectives: 107 us -> 0 us
  starting transfers between devices: 17.8 us -> 77.5 us
  Pallas kernels: 0 us -> 20.4 us
  waiting for transfers between devices: 166 us -> 174 us
  local copies, waits for them, and re-layouts: 3.16 us -> 8.9 us
    all_to_all x2 -> x0, blocking collectives: 107 us -> none  [exchange(): lax.all_to_all(value, 'fs', split_axis=0, concat_axis=0, tiled=True, axis...]
    ppermute x0 -> x9, waiting for transfers between devices: none -> 75.4 us  [the longest x6 44.2 us: along_line(): lax.ppermute(value, 'fs', [((z * inner + y) * copies + c, ((z + step) * i...]
    ppermute x3 -> x5, waiting for transfers between devices: 123 us -> 58.7 us  [hand_round(): lax.ppermute(value, 'fs', [(e * copies + c, e * copies + (c + step) % cop...]
    ppermute x0 -> x9, starting transfers between devices: none -> 35.2 us  [the longest x6 31.4 us: along_line(): lax.ppermute(value, 'fs', [((z * inner + y) * copies + c, ((z + step) * i...]
    all_to_all x3 -> x7, starting transfers between devices: 13.1 us -> 35.6 us  [exchange(): lax.all_to_all(value, 'fs', split_axis=0, concat_axis=0, tiled=True, axis...]
    pallas_call x0 -> x4, Pallas kernels: none -> 20.4 us  [the longest x3 15.4 us: place(): pl.pallas_call(functools.partial(place_kernel, moves, len(arrays)), grid_...]
    unnamed x10 -> x38, local copies, waits for them, and re-layouts: 0.02 us -> 5.13 us
    ppermute x3 -> x4, waiting for transfers between devices: 5.11 us -> 1.13 us  [other_core(): return lax.ppermute(value, 'tp', [(0, 1), (1, 0)])]
  transfers between devices with their start and end apart: 9 -> 25, of which waited for: 7 -> 13; matrix products, arithmetic and copies ran while one was open for 5% -> 14% of each run, Pallas kernels for 0% -> 6%
where the time goes in v2:
time: 332 us; the launch traced here: 331 us
  waiting for transfers between devices  174 us (52%)
  starting transfers between devices  77.5 us (23%)
  matrix products  24.7 us (7%)
  other arithmetic  23.8 us (7%)
  Pallas kernels  20.4 us (6%)
  local copies, waits for them, and re-layouts  8.9 us (3%)
    ppermute x5, waiting for transfers between devices, hand_round(): lax.ppermute(value, 'fs', [(e * copies + c, e * copies + (c + step) % cop...  58.7 us
    ppermute x6, waiting for transfers between devices, along_line(): lax.ppermute(value, 'fs', [((z * inner + y) * copies + c, ((z + step) * i...  44.2 us
    all_to_all x7, waiting for transfers between devices, exchange(): lax.all_to_all(value, 'fs', split_axis=0, concat_axis=0, tiled=True, axis...  39.1 us
    all_to_all x7, starting transfers between devices, exchange(): lax.all_to_all(value, 'fs', split_axis=0, concat_axis=0, tiled=True, axis...  35.6 us
    ppermute x6, starting transfers between devices, along_line(): lax.ppermute(value, 'fs', [((z * inner + y) * copies + c, ((z + step) * i...  31.4 us
    ppermute x3, waiting for transfers between devices, across(): lax.ppermute(value, 'fs', [((z * inner + y) * copies + c, (z * inner + 1...  31.2 us
    pallas_call x3, Pallas kernels, place(): pl.pallas_call(functools.partial(place_kernel, moves, len(arrays)), grid_...  15.4 us
    dot_general x1, matrix products, body(): up_act = jnp.dot(piece, up_new[0], preferred_element_type=jnp.float32)  8.66 us
  transfers between devices with their start and end apart: 25, of which 13 were waited for; matrix products, arithmetic and copies ran while one was open for 14% of the time, Pallas kernels for 6%

profile of v2, /device:TPU:0, one launch (start us, length us, event | category | flops | bytes accessed | tf_op | source)
XLA Modules:
  0.0 330.7 jit_solution(18053893068911227447)
XLA Ops:
  0.6 3.0 multiply_convert_fusion.3
  3.6 7.3 %all-to-all-start = ((bf16[8,64,1024]{2,1,0:T(8,128)(2,1)}), bf16[8,64,1024]{2,1,0:T(8,128)(2,1)}, u32[]{:S(2)}, u32[]{:S(2)}) async-start(bf16[8,64,1024]{2,1,0:T(8,128)(2,1)} %multiply_convert_fusion.3), calls=%async_computation | async-start | bytes 2097152 | tf_op jit(solution)/shard_map/all_to_all | solution.py:111
  13.1 2.2 multiply_convert_fusion.4
  15.6 1.4 pad_maximum_fusion
  17.0 19.8 %all-to-all-done.refs_0_ = bf16[8,64,1024]{2,1,0:T(8,128)(2,1)} async-done(((bf16[8,64,1024]{2,1,0:T(8,128)(2,1)}), bf16[8,64,1024]{2,1,0:T(8,128)(2,1)}, u32[]{:S(2)}, u32[]{:S(2)}) %all-to-all-start) | async-done | bytes 1048608 | tf_op jit(solution)/shard_map/all_to_all | solution.py:111
  36.8 3.6 %all-to-all-start.1 = ((bf16[8,112,1024]{2,1,0:T(8,128)(2,1)}), bf16[8,112,1024]{2,1,0:T(8,128)(2,1)S(1)}, u32[]{:S(2)}, u32[]{:S(2)}) async-start(bf16[8,112,1024]{2,1,0:T(8,128)(2,1)} %pad_maximum_fusion), calls=%async_computation.1 | async-start | bytes 3670016 | tf_op jit(solution)/shard_map/all_to_all | solution.py:111
  40.4 1.3 collective-permute-start.2
  41.7 4.6 %collective-permute-start = (bf16[192,1152]{1,0:T(8,128)(2,1)S(1)}, bf16[192,1152]{1,0:T(8,128)(2,1)S(1)}, u32[]{:S(2)}, u32[]{:S(2)}) collective-permute-start(bf16[192,1152]{1,0:T(8,128)(2,1)S(1)} %get-tuple-element.53), channel_id=1, source_target_pairs={{0,8},{2,10},{4,12},{6,14},{8,16},{10,18},{12,20},{14,22},{16,24},... | collective-permute-start | bytes 1327112 | tf_op jit(solution)/shard_map/ppermute | solution.py:184
  46.3 26.9 %collective-permute-done.2 = bf16[192,1152]{1,0:T(8,128)(2,1)S(1)} collective-permute-done((bf16[192,1152]{1,0:T(8,128)(2,1)S(1)}, bf16[192,1152]{1,0:T(8,128)(2,1)S(1)}, u32[]{:S(2)}, u32[]{:S(2)}) %collective-permute-start.2) | collective-permute-done | bytes 442400 | tf_op jit(solution)/shard_map/ppermute | solution.py:184
  74.0 1.3 collective-permute-start.3
  75.3 5.6 %collective-permute-done = bf16[192,1152]{1,0:T(8,128)(2,1)S(1)} collective-permute-done((bf16[192,1152]{1,0:T(8,128)(2,1)S(1)}, bf16[192,1152]{1,0:T(8,128)(2,1)S(1)}, u32[]{:S(2)}, u32[]{:S(2)}) %collective-permute-start) | collective-permute-done | bytes 442400 | tf_op jit(solution)/shard_map/ppermute | solution.py:184
  80.9 17.7 %collective-permute-start.1 = (bf16[192,1152]{1,0:T(8,128)(2,1)S(1)}, bf16[192,1152]{1,0:T(8,128)(2,1)}, u32[]{:S(2)}, u32[]{:S(2)}) collective-permute-start(bf16[192,1152]{1,0:T(8,128)(2,1)S(1)} %collective-permute-done), channel_id=1, source_target_pairs={{0,8},{2,10},{4,12},{6,14},{8,16},{10,18},{12,20},{14,22},{16,24},... | collective-permute-start | bytes 1327112 | tf_op jit(solution)/shard_map/ppermute | solution.py:184
  98.6 6.5 %collective-permute-done.3 = bf16[192,1152]{1,0:T(8,128)(2,1)S(1)} collective-permute-done((bf16[192,1152]{1,0:T(8,128)(2,1)S(1)}, bf16[192,1152]{1,0:T(8,128)(2,1)S(1)}, u32[]{:S(2)}, u32[]{:S(2)}) %collective-permute-start.3) | collective-permute-done | bytes 442400 | tf_op jit(solution)/shard_map/ppermute | solution.py:184
  105.1 1.3 collective-permute-start.4
  106.4 1.7 collective-permute-start.6
  108.2 3.2 multiply_convert_fusion.1
  111.4 5.3 %collective-permute-start.5 = (bf16[192,1152]{1,0:T(8,128)(2,1)}, bf16[192,1152]{1,0:T(8,128)(2,1)}, u32[]{:S(2)}, u32[]{:S(2)}) collective-permute-start(bf16[192,1152]{1,0:T(8,128)(2,1)} %collective-permute-done.1), channel_id=1, source_target_pairs={{0,8},{2,10},{4,12},{6,14},{8,16},{10,18},{12,20},{14,22},{16,24},... | collective-permute-start | bytes 1327112 | tf_op jit(solution)/shard_map/ppermute | solution.py:184
  118.3 4.1 %all-to-all-start.2 = ((bf16[8,80,1024]{2,1,0:T(8,128)(2,1)}), bf16[8,80,1024]{2,1,0:T(8,128)(2,1)S(1)}, u32[]{:S(2)}, u32[]{:S(2)}) async-start(bf16[8,80,1024]{2,1,0:T(8,128)(2,1)} %multiply_convert_fusion.1), calls=%async_computation.2 | async-start | bytes 2621440 | tf_op jit(solution)/shard_map/all_to_all | solution.py:111
  122.4 4.4 %collective-permute-done.5 = bf16[192,1152]{1,0:T(8,128)(2,1)} collective-permute-done((bf16[192,1152]{1,0:T(8,128)(2,1)}, bf16[192,1152]{1,0:T(8,128)(2,1)}, u32[]{:S(2)}, u32[]{:S(2)}) %collective-permute-start.5) | collective-permute-done | bytes 442400 | tf_op jit(solution)/shard_map/ppermute | solution.py:184
  127.9 2.0 pad_maximum_fusion.5.refs_2_
  130.7 2.0 collective-permute-start.7
  132.7 1.5 collective-permute-start.11
  134.8 31.1 %collective-permute-done.7 = bf16[192,1152]{1,0:T(8,128)(2,1)} collective-permute-done((bf16[192,1152]{1,0:T(8,128)(2,1)}, bf16[192,1152]{1,0:T(8,128)(2,1)}, u32[]{:S(2)}, u32[]{:S(2)}) %collective-permute-start.7) | collective-permute-done | bytes 442400 | tf_op jit(solution)/shard_map/ppermute | solution.py:197
  166.0 5.0 %shard_map.102 = bf16[8,96,1024]{2,1,0:T(8,128)(2,1)} custom-call(s32[9]{0:T(128)} %stack.99.where_ref, bf16[1,192,1152]{2,1,0:T(8,128)(2,1)} %get-tuple-element.52.refs_0_, bf16[1,192,1152]{2,1,0:T(8,128)(2,1)} %bitcast.12.refs_1_, bf16[2,192,1152]{2,1,0:T(8,128)(2,1)} %pad_maximum_fusion.5.refs_2_, bf16[1,192,1152]{2,1,0:T(8,128)(2,1)} %bitcast.15.refs_3_, ...), custom_call_target="tpu_custom_call" | custom-call | flops 301989888 | bytes 7077888 | tf_op jit(solution)/shard_map/pallas_call | solution.py:86
  171.0 2.5 convert.4
  173.5 1.6 collective-permute-start.10
  175.1 1.7 fusion.26
  176.7 1.2 copy-done.3
  177.9 4.6 %all-to-all-start.3 = ((bf16[8,64,1024]{2,1,0:T(8,128)(2,1)}), bf16[8,64,1024]{2,1,0:T(8,128)(2,1)S(1)}, u32[]{:S(2)}, u32[]{:S(2)}) async-start(bf16[8,64,1024]{2,1,0:T(8,128)(2,1)} %get-tuple-element.27), calls=%async_computation.3 | async-start | bytes 2097152 | tf_op jit(solution)/shard_map/all_to_all | solution.py:111
  183.6 16.3 %collective-permute-done.10.refs_1_ = bf16[8,64,1024]{2,1,0:T(8,128)(2,1)} collective-permute-done((bf16[8,64,1024]{2,1,0:T(8,128)(2,1)}, bf16[8,64,1024]{2,1,0:T(8,128)(2,1)}, u32[]{:S(2)}, u32[]{:S(2)}) %collective-permute-start.10) | collective-permute-done | bytes 1048608 | tf_op jit(solution)/shard_map/ppermute | solution.py:117
  199.9 5.9 %shard_map.103 = bf16[16,128,1024]{2,1,0:T(8,128)(2,1)} custom-call(s32[16]{0:T(128)} %stack.119.where_ref, bf16[8,64,1024]{2,1,0:T(8,128)(2,1)} %all-to-all-done.refs_0_, bf16[8,64,1024]{2,1,0:T(8,128)(2,1)} %collective-permute-done.10.refs_1_, bf16[8,112,1024]{2,1,0:T(8,128)(2,1)} %copy-done, bf16[8,112,1024]{2,1,0:T(8,128)(2,1)} %collective-permute-done.11.refs_3_.refs_1_), custom_call_target="tpu_custom_call" | custom-call | flops 23068672 | bytes 11534336 | tf_op jit(solution)/shard_map/pallas_call | solution.py:48
  205.8 8.2 %fusion.11 = f32[768,1024]{1,0:T(8,128)} fusion(bf16[2048,1024]{1,0:T(8,128)(2,1)} %bitcast.73, bf16[768,1024]{1,0:T(8,128)(2,1)} %collective-permute-done.9, bf16[768,1024]{1,0:T(8,128)(2,1)S(1)} %bitcast.81, pred[]{:T(512)S(6)} %eq.116), kind=kOutput, calls=%fused_computation.43 | convolution fusion | flops 3235381248 | bytes 10485761 | tf_op jit(solution)/shard_map/dot_general | solution.py:268
  214.1 13.5 %collective-permute-done.12.refs_3_ = bf16[8,80,1024]{2,1,0:T(8,128)(2,1)} collective-permute-done((bf16[8,80,1024]{2,1,0:T(8,128)(2,1)}, bf16[8,80,1024]{2,1,0:T(8,128)(2,1)}, u32[]{:S(2)}, u32[]{:S(2)}) %collective-permute-start.12) | collective-permute-done | bytes 1310752 | tf_op jit(solution)/shard_map/ppermute | solution.py:117
  227.5 5.3 %shard_map.104 = bf16[16,128,1024]{2,1,0:T(8,128)(2,1)} custom-call(s32[16]{0:T(128)} %stack.119.where_ref, bf16[8,112,1024]{2,1,0:T(8,128)(2,1)} %copy-done, bf16[8,112,1024]{2,1,0:T(8,128)(2,1)} %collective-permute-done.11.refs_3_.refs_1_, bf16[8,80,1024]{2,1,0:T(8,128)(2,1)} %copy-done.3, bf16[8,80,1024]{2,1,0:T(8,128)(2,1)} %collective-permute-done.12.refs_3_), custom_call_target="tpu_custom_call" | custom-call | flops 25165824 | bytes 12582912 | tf_op jit(solution)/shard_map/pallas_call | solution.py:48
  232.9 4.6 %all-to-all-start.4 = ((bf16[8,64,1024]{2,1,0:T(8,128)(2,1)}), bf16[8,64,1024]{2,1,0:T(8,128)(2,1)S(1)}, u32[]{:S(2)}, u32[]{:S(2)}) async-start(bf16[8,64,1024]{2,1,0:T(8,128)(2,1)} %get-tuple-element.32), calls=%async_computation.4 | async-start | bytes 2097152 | tf_op jit(solution)/shard_map/all_to_all | solution.py:111
  237.5 1.5 collective-permute-start.13
  238.9 8.7 %multiply_convert_fusion = bf16[768,1024]{1,0:T(8,128)(2,1)S(1)} fusion(f32[768,1024]{1,0:T(8,128)} %fusion.11, bf16[2048,1024]{1,0:T(8,128)(2,1)} %bitcast.75, bf16[768,1024]{1,0:T(8,128)(2,1)} %collective-permute-done.9, bf16[768,1024]{1,0:T(8,128)(2,1)} %bitcast.80, pred[]{:T(512)S(6)} %eq.116), kind=kOutput, calls=%fused_computation.3 | convolution fusion | flops 3240099840 | bytes 12058625 | tf_op jit(solution)/shard_map/dot_general | solution.py:269
  247.7 14.1 %collective-permute-done.13.refs_1_ = bf16[8,64,1024]{2,1,0:T(8,128)(2,1)S(1)} collective-permute-done((bf16[8,64,1024]{2,1,0:T(8,128)(2,1)S(1)}, bf16[8,64,1024]{2,1,0:T(8,128)(2,1)S(1)}, u32[]{:S(2)}, u32[]{:S(2)}) %collective-permute-start.13) | collective-permute-done | bytes 1048608 | tf_op jit(solution)/shard_map/ppermute | solution.py:117
  262.9 1.9 convolution_convert_fusion.2
  264.8 1.6 collective-permute-start.15
  267.6 2.3 add_convert_fusion.1
  269.9 5.7 %all-to-all-start.5 = ((bf16[8,96,512]{2,1,0:T(8,128)(2,1)}), bf16[8,96,512]{2,1,0:T(8,128)(2,1)S(1)}, u32[]{:S(2)}, u32[]{:S(2)}) async-start(bf16[8,96,512]{2,1,0:T(8,128)(2,1)} %bitcast.78), calls=%async_computation.5 | async-start | bytes 1572864 | tf_op jit(solution)/shard_map/all_to_all | solution.py:111
  275.6 14.8 %collective-permute-done.15.refs_3_ = bf16[8,64,1024]{2,1,0:T(8,128)(2,1)S(1)} collective-permute-done((bf16[8,64,1024]{2,1,0:T(8,128)(2,1)S(1)}, bf16[8,64,1024]{2,1,0:T(8,128)(2,1)S(1)}, u32[]{:S(2)}, u32[]{:S(2)}) %collective-permute-start.15) | collective-permute-done | bytes 1048608 | tf_op jit(solution)/shard_map/ppermute | solution.py:117
  291.4 1.3 copy-done.18
  297.2 5.7 %all-to-all-start.6 = ((bf16[8,96,512]{2,1,0:T(8,128)(2,1)}), bf16[8,96,512]{2,1,0:T(8,128)(2,1)S(1)}, u32[]{:S(2)}, u32[]{:S(2)}) async-start(bf16[8,96,512]{2,1,0:T(8,128)(2,1)} %bitcast.44), calls=%async_computation.6 | async-start | bytes 1572864 | tf_op jit(solution)/shard_map/all_to_all | solution.py:111
  304.1 19.3 %all-to-all-done.6 = bf16[8,96,512]{2,1,0:T(8,128)(2,1)S(1)} async-done(((bf16[8,96,512]{2,1,0:T(8,128)(2,1)}), bf16[8,96,512]{2,1,0:T(8,128)(2,1)S(1)}, u32[]{:S(2)}, u32[]{:S(2)}) %all-to-all-start.6) | async-done | bytes 786464 | tf_op jit(solution)/shard_map/all_to_all | solution.py:111
  325.4 4.2 %shard_map.105 = bf16[16,128,1024]{2,1,0:T(8,128)(2,1)} custom-call(s32[16]{0:T(128)} %stack.119.where_ref, bf16[8,64,1024]{2,1,0:T(8,128)(2,1)} %copy-done.2, bf16[8,64,1024]{2,1,0:T(8,128)(2,1)} %copy-done.5, bf16[8,64,1024]{2,1,0:T(8,128)(2,1)} %copy-done.1, bf16[8,64,1024]{2,1,0:T(8,128)(2,1)} %copy-done.4), custom_call_target="tpu_custom_call" | custom-call | flops 16777216 | bytes 8388608 | tf_op jit(solution)/shard_map/pallas_call | solution.py:48
  329.6 1.2 maximum_select_fusion.1
  (99 shorter events, 19.5 us)
Async XLA Ops:
  0.6 10.3 %copy-start.7 = (bf16[192,2048]{1,0:T(8,128)(2,1)S(1)}, bf16[192,2048]{1,0:T(8,128)(2,1)}, u32[]{:S(2)}) copy-start(bf16[192,2048]{1,0:T(8,128)(2,1)} %param.7) | copy-start | bytes 2359300
  3.6 33.2 %all-to-all-start = ((bf16[8,64,1024]{2,1,0:T(8,128)(2,1)}), bf16[8,64,1024]{2,1,0:T(8,128)(2,1)}, u32[]{:S(2)}, u32[]{:S(2)}) async-start(bf16[8,64,1024]{2,1,0:T(8,128)(2,1)} %multiply_convert_fusion.3), calls=%async_computation | async-start | bytes 2097152 | tf_op jit(solution)/shard_map/all_to_all | solution.py:111
  10.9 0.7 copy-start.13
  11.1 1.9 copy-start.15
  12.1 3.2 copy-start.6
  13.0 28.6 %copy-start.12 = (bf16[192,1152]{1,0:T(8,128)(2,1)}, bf16[192,1152]{1,0:T(8,128)(2,1)S(1)}, u32[]{:S(2)}) copy-start(bf16[192,1152]{1,0:T(8,128)(2,1)S(1)} %get-tuple-element.53) | copy-start | bytes 1327108
  36.8 81.5 %all-to-all-start.1 = ((bf16[8,112,1024]{2,1,0:T(8,128)(2,1)}), bf16[8,112,1024]{2,1,0:T(8,128)(2,1)S(1)}, u32[]{:S(2)}, u32[]{:S(2)}) async-start(bf16[8,112,1024]{2,1,0:T(8,128)(2,1)} %pad_maximum_fusion), calls=%async_computation.1 | async-start | bytes 3670016 | tf_op jit(solution)/shard_map/all_to_all | solution.py:111
  40.4 32.8 %collective-permute-start.2 = (bf16[192,1152]{1,0:T(8,128)(2,1)S(1)}, bf16[192,1152]{1,0:T(8,128)(2,1)S(1)}, u32[]{:S(2)}, u32[]{:S(2)}) collective-permute-start(bf16[192,1152]{1,0:T(8,128)(2,1)S(1)} %get-tuple-element.53), channel_id=1, source_target_pairs={{8,0},{10,2},{12,4},{14,6},{16,8},{18,10},{20,12},{22,14},{24,16},... | collective-permute-start | bytes 1327112 | tf_op jit(solution)/shard_map/ppermute | solution.py:184
  41.7 39.2 %collective-permute-start = (bf16[192,1152]{1,0:T(8,128)(2,1)S(1)}, bf16[192,1152]{1,0:T(8,128)(2,1)S(1)}, u32[]{:S(2)}, u32[]{:S(2)}) collective-permute-start(bf16[192,1152]{1,0:T(8,128)(2,1)S(1)} %get-tuple-element.53), channel_id=1, source_target_pairs={{0,8},{2,10},{4,12},{6,14},{8,16},{10,18},{12,20},{14,22},{16,24},... | collective-permute-start | bytes 1327112 | tf_op jit(solution)/shard_map/ppermute | solution.py:184
  73.2 0.8 copy-start.9
  74.0 31.1 %collective-permute-start.3 = (bf16[192,1152]{1,0:T(8,128)(2,1)S(1)}, bf16[192,1152]{1,0:T(8,128)(2,1)S(1)}, u32[]{:S(2)}, u32[]{:S(2)}) collective-permute-start(bf16[192,1152]{1,0:T(8,128)(2,1)S(1)} %collective-permute-done.2), channel_id=1, source_target_pairs={{8,0},{10,2},{12,4},{14,6},{16,8},{18,10},{20,12},{22,14},{24,16},... | collective-permute-start | bytes 1327112 | tf_op jit(solution)/shard_map/ppermute | solution.py:184
  80.9 30.5 %collective-permute-start.1 = (bf16[192,1152]{1,0:T(8,128)(2,1)S(1)}, bf16[192,1152]{1,0:T(8,128)(2,1)}, u32[]{:S(2)}, u32[]{:S(2)}) collective-permute-start(bf16[192,1152]{1,0:T(8,128)(2,1)S(1)} %collective-permute-done), channel_id=1, source_target_pairs={{0,8},{2,10},{4,12},{6,14},{8,16},{10,18},{12,20},{14,22},{16,24},... | collective-permute-start | bytes 1327112 | tf_op jit(solution)/shard_map/ppermute | solution.py:184
  105.1 13.1 %copy-start.10 = (bf16[192,1152]{1,0:T(8,128)(2,1)}, bf16[192,1152]{1,0:T(8,128)(2,1)S(1)}, u32[]{:S(2)}) copy-start(bf16[192,1152]{1,0:T(8,128)(2,1)S(1)} %collective-permute-done.3) | copy-start | bytes 1327108
  105.1 12.3 %collective-permute-start.4 = (bf16[192,1152]{1,0:T(8,128)(2,1)S(1)}, bf16[192,1152]{1,0:T(8,128)(2,1)S(1)}, u32[]{:S(2)}, u32[]{:S(2)}) collective-permute-start(bf16[192,1152]{1,0:T(8,128)(2,1)S(1)} %collective-permute-done.3), channel_id=1, source_target_pairs={{8,0},{10,2},{12,4},{14,6},{16,8},{18,10},{20,12},{22,14},{24,16},... | collective-permute-start | bytes 1327112 | tf_op jit(solution)/shard_map/ppermute | solution.py:184
  106.4 28.4 %collective-permute-start.6 = (bf16[192,1152]{1,0:T(8,128)(2,1)}, bf16[192,1152]{1,0:T(8,128)(2,1)}, u32[]{:S(2)}, u32[]{:S(2)}) collective-permute-start(bf16[192,1152]{1,0:T(8,128)(2,1)} %copy-done.12), channel_id=1, source_target_pairs={{0,4},{2,6},{4,0},{6,2},{8,12},{10,14},{12,8},{14,10},{16,20},{18,... | collective-permute-start | bytes 1327112 | tf_op jit(solution)/shard_map/ppermute | solution.py:197
  111.4 15.4 %collective-permute-start.5 = (bf16[192,1152]{1,0:T(8,128)(2,1)}, bf16[192,1152]{1,0:T(8,128)(2,1)}, u32[]{:S(2)}, u32[]{:S(2)}) collective-permute-start(bf16[192,1152]{1,0:T(8,128)(2,1)} %collective-permute-done.1), channel_id=1, source_target_pairs={{0,8},{2,10},{4,12},{6,14},{8,16},{10,18},{12,20},{14,22},{16,24},... | collective-permute-start | bytes 1327112 | tf_op jit(solution)/shard_map/ppermute | solution.py:184
  118.3 14.5 %copy-start = (bf16[8,112,1024]{2,1,0:T(8,128)(2,1)}, bf16[8,112,1024]{2,1,0:T(8,128)(2,1)S(1)}, u32[]{:S(2)}) copy-start(bf16[8,112,1024]{2,1,0:T(8,128)(2,1)S(1)} %all-to-all-done.1.refs_2_.refs_0_) | copy-start | bytes 5505028
  118.3 58.4 %all-to-all-start.2 = ((bf16[8,80,1024]{2,1,0:T(8,128)(2,1)}), bf16[8,80,1024]{2,1,0:T(8,128)(2,1)S(1)}, u32[]{:S(2)}, u32[]{:S(2)}) async-start(bf16[8,80,1024]{2,1,0:T(8,128)(2,1)} %multiply_convert_fusion.1), calls=%async_computation.2 | async-start | bytes 2621440 | tf_op jit(solution)/shard_map/all_to_all | solution.py:111
  122.4 7.5 %copy-start.11 = (bf16[192,1152]{1,0:T(8,128)(2,1)S(1)}, bf16[192,1152]{1,0:T(8,128)(2,1)}, u32[]{:S(2)}) copy-start(bf16[192,1152]{1,0:T(8,128)(2,1)} %copy-done.10) | copy-start | bytes 1327108
  129.9 36.1 %collective-permute-start.8 = (bf16[2,192,1152]{2,1,0:T(8,128)(2,1)}, bf16[2,192,1152]{2,1,0:T(8,128)(2,1)}, u32[]{:S(2)}, u32[]{:S(2)}) collective-permute-start(bf16[2,192,1152]{2,1,0:T(8,128)(2,1)} %pad_maximum_fusion.5.refs_2_), channel_id=1, source_target_pairs={{0,4},{2,6},{4,0},{6,2},{8,12},{10,14},{12,8},{14,10},{16,20},{18,... | collective-permute-start | bytes 2654216 | tf_op jit(solution)/shard_map/ppermute | solution.py:197
  130.7 35.3 %collective-permute-start.7 = (bf16[192,1152]{1,0:T(8,128)(2,1)}, bf16[192,1152]{1,0:T(8,128)(2,1)}, u32[]{:S(2)}, u32[]{:S(2)}) collective-permute-start(bf16[192,1152]{1,0:T(8,128)(2,1)} %broadcast_select_fusion), channel_id=1, source_target_pairs={{0,4},{2,6},{4,0},{6,2},{8,12},{10,14},{12,8},{14,10},{16,20},{18,... | collective-permute-start | bytes 1327112 | tf_op jit(solution)/shard_map/ppermute | solution.py:197
  132.7 67.2 %collective-permute-start.11 = (bf16[8,112,1024]{2,1,0:T(8,128)(2,1)S(1)}, bf16[8,112,1024]{2,1,0:T(8,128)(2,1)}, u32[]{:S(2)}, u32[]{:S(2)}) collective-permute-start(bf16[8,112,1024]{2,1,0:T(8,128)(2,1)S(1)} %all-to-all-done.1.refs_2_.refs_0_), channel_id=1, source_target_pairs={{0,2},{2,0},{4,6},{6,4},{8,10},{10,8},{12,14},{14,12},{16,18},{18,... | collective-permute-start | bytes 5505032 | tf_op jit(solution)/shard_map/ppermute | solution.py:117
  171.0 34.8 %collective-permute-start.9 = (bf16[768,1024]{1,0:T(8,128)(2,1)}, bf16[768,1024]{1,0:T(8,128)(2,1)}, u32[]{:S(2)}, u32[]{:S(2)}) collective-permute-start(bf16[768,1024]{1,0:T(8,128)(2,1)} %bitcast.79), channel_id=1, source_target_pairs={{0,1},{1,0},{2,3},{3,2},{4,5},{5,4},{6,7},{7,6},{8,9},{9,8},{10,11... | collective-permute-start | bytes 4718600 | tf_op jit(solution)/shard_map/ppermute | solution.py:130
  173.5 26.4 %collective-permute-start.10 = (bf16[8,64,1024]{2,1,0:T(8,128)(2,1)}, bf16[8,64,1024]{2,1,0:T(8,128)(2,1)}, u32[]{:S(2)}, u32[]{:S(2)}) collective-permute-start(bf16[8,64,1024]{2,1,0:T(8,128)(2,1)} %all-to-all-done.refs_0_), channel_id=1, source_target_pairs={{0,2},{2,0},{4,6},{6,4},{8,10},{10,8},{12,14},{14,12},{16,18},{18,... | collective-permute-start | bytes 3145736 | tf_op jit(solution)/shard_map/ppermute | solution.py:117
  176.7 1.2 copy-start.3
  177.9 55.0 %all-to-all-start.3 = ((bf16[8,64,1024]{2,1,0:T(8,128)(2,1)}), bf16[8,64,1024]{2,1,0:T(8,128)(2,1)S(1)}, u32[]{:S(2)}, u32[]{:S(2)}) async-start(bf16[8,64,1024]{2,1,0:T(8,128)(2,1)} %get-tuple-element.27), calls=%async_computation.3 | async-start | bytes 2097152 | tf_op jit(solution)/shard_map/all_to_all | solution.py:111
  182.4 45.1 %collective-permute-start.12 = (bf16[8,80,1024]{2,1,0:T(8,128)(2,1)}, bf16[8,80,1024]{2,1,0:T(8,128)(2,1)}, u32[]{:S(2)}, u32[]{:S(2)}) collective-permute-start(bf16[8,80,1024]{2,1,0:T(8,128)(2,1)} %copy-done.3), channel_id=1, source_target_pairs={{0,2},{2,0},{4,6},{6,4},{8,10},{10,8},{12,14},{14,12},{16,18},{18,... | collective-permute-start | bytes 3932168 | tf_op jit(solution)/shard_map/ppermute | solution.py:117
  199.9 5.9 %copy-start.8 = (bf16[8,96,1024]{2,1,0:T(8,128)(2,1)S(1)}, bf16[8,96,1024]{2,1,0:T(8,128)(2,1)}, u32[]{:S(2)}) copy-start(bf16[8,96,1024]{2,1,0:T(8,128)(2,1)} %shard_map.102) | copy-start | bytes 4718596
  232.9 14.7 %copy-start.2 = (bf16[8,64,1024]{2,1,0:T(8,128)(2,1)}, bf16[8,64,1024]{2,1,0:T(8,128)(2,1)S(1)}, u32[]{:S(2)}) copy-start(bf16[8,64,1024]{2,1,0:T(8,128)(2,1)S(1)} %all-to-all-done.3.refs_0_) | copy-start | bytes 3145732
  232.9 31.9 %all-to-all-start.4 = ((bf16[8,64,1024]{2,1,0:T(8,128)(2,1)}), bf16[8,64,1024]{2,1,0:T(8,128)(2,1)S(1)}, u32[]{:S(2)}, u32[]{:S(2)}) async-start(bf16[8,64,1024]{2,1,0:T(8,128)(2,1)} %get-tuple-element.32), calls=%async_computation.4 | async-start | bytes 2097152 | tf_op jit(solution)/shard_map/all_to_all | solution.py:111
  237.5 24.4 %collective-permute-start.13 = (bf16[8,64,1024]{2,1,0:T(8,128)(2,1)S(1)}, bf16[8,64,1024]{2,1,0:T(8,128)(2,1)S(1)}, u32[]{:S(2)}, u32[]{:S(2)}) collective-permute-start(bf16[8,64,1024]{2,1,0:T(8,128)(2,1)S(1)} %all-to-all-done.3.refs_0_), channel_id=1, source_target_pairs={{0,2},{2,0},{4,6},{6,4},{8,10},{10,8},{12,14},{14,12},{16,18},{18,... | collective-permute-start | bytes 3145736 | tf_op jit(solution)/shard_map/ppermute | solution.py:117
  247.6 15.3 %copy-start.16 = (bf16[768,1024]{1,0:T(8,128)(2,1)}, bf16[768,1024]{1,0:T(8,128)(2,1)S(1)}, u32[]{:S(2)}) copy-start(bf16[768,1024]{1,0:T(8,128)(2,1)S(1)} %multiply_convert_fusion) | copy-start | bytes 4718596
  261.9 1.0 copy-start.5
  264.8 2.8 collective-permute-start.14
  264.8 25.6 %copy-start.1 = (bf16[8,64,1024]{2,1,0:T(8,128)(2,1)}, bf16[8,64,1024]{2,1,0:T(8,128)(2,1)S(1)}, u32[]{:S(2)}) copy-start(bf16[8,64,1024]{2,1,0:T(8,128)(2,1)S(1)} %all-to-all-done.4.refs_2_) | copy-start | bytes 3145732
  264.8 1.8 copy-start.17
  264.8 25.6 %collective-permute-start.15 = (bf16[8,64,1024]{2,1,0:T(8,128)(2,1)S(1)}, bf16[8,64,1024]{2,1,0:T(8,128)(2,1)S(1)}, u32[]{:S(2)}, u32[]{:S(2)}) collective-permute-start(bf16[8,64,1024]{2,1,0:T(8,128)(2,1)S(1)} %all-to-all-done.4.refs_2_), channel_id=1, source_target_pairs={{0,2},{2,0},{4,6},{6,4},{8,10},{10,8},{12,14},{14,12},{16,18},{18,... | collective-permute-start | bytes 3145736 | tf_op jit(solution)/shard_map/ppermute | solution.py:117
  269.9 27.4 %all-to-all-start.5 = ((bf16[8,96,512]{2,1,0:T(8,128)(2,1)}), bf16[8,96,512]{2,1,0:T(8,128)(2,1)S(1)}, u32[]{:S(2)}, u32[]{:S(2)}) async-start(bf16[8,96,512]{2,1,0:T(8,128)(2,1)} %bitcast.78), calls=%async_computation.5 | async-start | bytes 1572864 | tf_op jit(solution)/shard_map/all_to_all | solution.py:111
  290.4 1.0 copy-start.4
  291.3 1.4 copy-start.18
  293.8 2.4 collective-permute-start.16
  295.0 8.3 %copy-start.14 = (f32[192,2]{0,1:T(2,128)S(1)}, f32[192,2]{0,1:T(2,128)}, u32[]{:S(2)}) copy-start(f32[192,2]{0,1:T(2,128)} %param.9) | copy-start | bytes 4612
  297.2 26.2 %all-to-all-start.6 = ((bf16[8,96,512]{2,1,0:T(8,128)(2,1)}), bf16[8,96,512]{2,1,0:T(8,128)(2,1)S(1)}, u32[]{:S(2)}, u32[]{:S(2)}) async-start(bf16[8,96,512]{2,1,0:T(8,128)(2,1)} %bitcast.44), calls=%async_computation.6 | async-start | bytes 1572864 | tf_op jit(solution)/shard_map/all_to_all | solution.py:111
  325.3 4.3 %collective-permute-start.17 = (bf16[192,1024]{1,0:T(8,128)(2,1)S(1)}, bf16[192,1024]{1,0:T(8,128)(2,1)S(1)}, u32[]{:S(2)}, u32[]{:S(2)}) collective-permute-start(bf16[192,1024]{1,0:T(8,128)(2,1)S(1)} %fusion.2), channel_id=1, source_target_pairs={{0,1},{1,0},{2,3},{3,2},{4,5},{5,4},{6,7},{7,6},{8,9},{9,8},{10,11... | collective-permute-start | bytes 1179656 | tf_op jit(solution)/shard_map/ppermute | solution.py:130

commit v3 on v2

--- a/solution.py
+++ b/solution.py
@@ -139,7 +139,7 @@
             )
         return lax.all_gather(part, "tp", axis=1, tiled=True)
 
-    cuts = [2 * depth * k // 16 // 16 * 16 for k in (0, 4, 11, 16)]
+    cuts = [2 * depth * k // 16 // 16 * 16 for k in (0, 5, 11, 16)]
     spans = list(zip(cuts[:-1], cuts[1:]))
     sources = [gate_weight, up_weight]
 
@@ -161,6 +161,21 @@
 
     first_block = fold(spans[0])
     tokens, route_ids = lax.optimization_barrier((tokens, route_ids, first_block))[:2]
+    tokens, route_ids = lax.optimization_barrier((tokens, route_ids, first_block))[:2]
+    block_expert = np.tile(np.arange(experts, dtype=np.int32), copies)
+    block_copy = np.repeat(np.arange(copies, dtype=np.int32), experts)
+
+    def moves_of(groups, pieces):
+        arrays, moves = [], []
+        for n, first, size, start in pieces:
+            moves += [
+                (len(arrays) + c, e, first, size, 0, start, c * experts + e)
+                for c in range(copies)
+                for e in range(experts)
+            ]
+            arrays += groups[n]
+        return arrays, moves
+
     names = jnp.arange(experts, dtype=jnp.int32)
     named = jnp.any(route_ids[:, :, None] == names[None, None, :], axis=1)
     row_no = jnp.arange(rows, dtype=jnp.int32)
@@ -210,35 +225,35 @@
     for _ in range(1, line):
         rising.append(along_line(rising[-1], 1))
         falling.append(along_line(falling[-1], -1))
-
-    def near(k):
-        return jnp.where(spot_z >= k, rising[k], falling[line - k])
-
-    middle = line // 2
-    ends = [k for k in range(1, line) if k != middle]
-    near_middle = near(middle)
-    near_ends = jnp.stack([near(k) for k in ends])
-    arrays = [chunk[None], near_middle[None], near_ends]
+    sides = [chunk]
+    if line == 4:
+        table = np.array([[0, 1, 2, 3], [1, 0, 3, 2], [2, 1, 0, 3], [3, 2, 1, 0]], np.int32)
+        first, last = spot_z == 0, spot_z == line - 1
+        sides.append(jnp.where(first, falling[1], rising[1]))
+        low = spot_z < 2
+        high_value = after(rising[2], sides[1])
+        sides.append(jnp.where(low, falling[2], high_value))
+        top = after(rising[3], sides[1], sides[2])
+        outer = jnp.where(first, falling[3], jnp.where(last, top, falling[1]))
+        sides.append(outer)
+    else:
+        table = np.array([[(z - k) % line for k in range(line)] for z in range(line)], np.int32)
+        for k in range(1, line):
+            sides.append(jnp.where(spot_z >= k, rising[k], falling[line - k]))
+    arrays = [value[None] for value in sides]
+    lines = jnp.sum(jnp.where(jnp.arange(line)[:, None] == spot_z, table, 0), axis=0)
+    order = [lines * inner + spot_y]
     if inner == 2:
-        far_own = across(chunk)
-        far_middle = across(near_middle)
-        far_ends = across(near_ends)
-        arrays += [far_own[None], far_middle[None], far_ends]
-    layout = []
-    order = []
-    for g in range(inner):
-        for k in range(line):
-            at = 0 if k == 0 else 1 if k == middle else 2
-            layout.append((3 * g + at, ends.index(k) if at == 2 else 0))
-            order.append((spot_z - k) % line * inner + (spot_y if g == 0 else 1 - spot_y))
-    where = jnp.stack(order + [expert]).astype(jnp.int32)
+        for value in sides:
+            arrays.append(across(value)[None])
+        order.append(lines * inner + 1 - spot_y)
+    layout = [(n, 0) for n in range(len(arrays))]
+    where = jnp.concatenate(order + [expert[None]]).astype(jnp.int32)
     piece_cols = pick_rows(arrays, layout, where, share_width)
     piece_cols = piece_cols.reshape(experts * CAP, share_width)
     piece = join_cols(piece_cols)
 
-    spots = jnp.stack(
-        [e * copies + (lane - c) % copies for c in range(copies) for e in range(experts)]
-    ).astype(jnp.int32)
+    spots = (block_expert * copies + (lane - block_copy) % copies).astype(jnp.int32)
     shape = (fs_count, depth, cols)
     held = []
     for n, span in enumerate(spans):
@@ -249,19 +264,14 @@
         held.append([own] + hand_round(own))
     made = []
     for target in range(2):
-        parts = []
-        moves = []
+        pieces = []
         for n, span in enumerate(spans):
             first = 0
             for tensor, start, size in segments(*span):
                 if tensor == target:
-                    moves += [
-                        (len(parts) + c, e, first, size, 0, start, c * experts + e)
-                        for c in range(copies)
-                        for e in range(experts)
-                    ]
-                    parts += held[n]
+                    pieces.append((n, first, size, start))
                 first += size
+        parts, moves = moves_of(held, pieces)
         made += place(parts, moves, spots, [shape])
     gate_new, up_new = (m.reshape(1, width, cols) for m in made)
 
@@ -278,45 +288,53 @@
         send = after(send, groups[-1][0] if n else held[-1][0])
         own = exchange(send)
         groups.append([own] + hand_round(own))
-    moves = [
-        (g * copies + c, e, 0, stop - start, 0, start, c * experts + e)
-        for g, (start, stop) in enumerate(spans)
-        for c in range(copies)
-        for e in range(experts)
-    ]
-    (down_new,) = place([a for group in groups for a in group], moves, spots, [shape])
+    parts, moves = moves_of(
+        groups, [(g, 0, stop - start, start) for g, (start, stop) in enumerate(spans)]
+    )
+    (down_new,) = place(parts, moves, spots, [shape])
     down_new = down_new.reshape(1, width, cols)
 
     tenth = experts // tp_count
 
-    def project(group):
-        def part(index):
-            matrix = jnp.concatenate(
-                [lax.dynamic_slice_in_dim(a, index * tenth, tenth, 0) for a in group], axis=0
-            ).reshape(-1, cols)
-            return jnp.einsum(
-                "rf,df->rd", hidden, matrix, preferred_element_type=jnp.float32
-            ).astype(jnp.bfloat16)
-
+    def times(matrix):
+        return jnp.einsum(
+            "rf,df->rd", hidden, matrix.reshape(-1, cols), preferred_element_type=jnp.float32
+        ).astype(jnp.bfloat16)
+
+    def shared(part, *earlier):
         if tp_count == 2:
-            given = part(1 - tp_index)
+            given = times(part(1 - tp_index, *earlier))
             came = other_core(given)
-            kept = after(part(tp_index), given)
-            share = (kept.astype(jnp.float32) + came.astype(jnp.float32)).astype(
-                jnp.bfloat16
-            )
+            kept = after(times(part(tp_index, given)), given)
+            share = (kept.astype(jnp.float32) + came.astype(jnp.float32)).astype(jnp.bfloat16)
         else:
-            partial = jnp.concatenate([part(t) for t in range(tp_count)], axis=1)
+            partial = jnp.concatenate([times(part(t)) for t in range(tp_count)], axis=1)
             share = lax.psum_scatter(partial, "tp", scatter_dimension=1, tiled=True)
         return share.reshape(experts, CAP, -1)
 
-    backs = []
-    shares = [hidden]
-    for n, group in enumerate(groups):
-        group = [after(a, shares[-1]) for a in group]
-        shares.append(project(group))
-        share = after(shares[-1], backs[-1] if n else groups[-1][0])
-        backs.append(exchange(share))
+    def blocks(copy_range, index, *earlier):
+        return jnp.concatenate(
+            [
+                lax.dynamic_slice_in_dim(
+                    after(group[c], *earlier) if earlier else group[c], index * tenth, tenth, 0
+                ).reshape(-1, cols)
+                for group in groups
+                for c in copy_range
+            ]
+        )
+
+    def own_part(index, *earlier):
+        return blocks(range(1), index)
+
+    def rest_part(index, *earlier):
+        return blocks(range(1, copies), index, *earlier)
+
+    share_own = shared(own_part)
+    share_own = after(share_own, groups[-1][0])
+    back_own = exchange(share_own)
+    share_rest = after(shared(rest_part, share_own), back_own)
+    back_rest = exchange(share_rest)
+    backs = [back_own, back_rest]
 
     def hot_rows(k):
         spot = jnp.sum(
@@ -341,12 +359,13 @@
             (
                 (
                     (jnp.arange(tenth)[None, :, None] * copies)
-                    + (lane - jnp.arange(copies)[:, None, None]) % copies
+                    + (lane - jnp.arange(lo, hi)[:, None, None]) % copies
                 )
                 * depth
                 + start
                 + jnp.arange(stop - start)[None, None, :]
             ).reshape(-1)
+            for lo, hi in ((0, 1), (1, copies))
             for start, stop in spans
         ]
     )

time: 332 us -> 363 us (1.093)
  waiting for transfers between devices: 174 us -> 210 us
    all_to_all x7, waiting for transfers between devices: 39.1 us -> 78.2 us  [exchange(): lax.all_to_all(value, 'fs', split_axis=0, concat_axis=0, tiled=True, axis...]
    ppermute x5, waiting for transfers between devices: 58.7 us -> 86.6 us  [hand_round(): lax.ppermute(value, 'fs', [(e * copies + c, e * copies + (c + step) % cop...]
    ppermute x3 -> x4, waiting for transfers between devices: 31.2 us -> 10.4 us  [across(): lax.ppermute(value, 'fs', [((z * inner + y) * copies + c, (z * inner + 1...]
    ppermute x6, waiting for transfers between devices: 44.2 us -> 34.5 us  [along_line(): lax.ppermute(value, 'fs', [((z * inner + y) * copies + c, ((z + step) * i...]
    ppermute x6, starting transfers between devices: 31.4 us -> 24.1 us  [along_line(): lax.ppermute(value, 'fs', [((z * inner + y) * copies + c, ((z + step) * i...]
    ppermute x3 -> x4, starting transfers between devices: 3.74 us -> 8.48 us  [across(): lax.ppermute(value, 'fs', [((z * inner + y) * copies + c, (z * inner + 1...]
    another operation x4 -> x1, other arithmetic: 6.43 us -> 2.51 us  [the longest x3 3.92 us: body(): near_ends = jnp.stack([near(k) for k in ends])]
  transfers between devices with their start and end apart: 25 -> 26, of which waited for: 13 -> 12; matrix products, arithmetic and copies ran while one was open for 14% -> 13% of each run, Pallas kernels for 6% -> 6%
where the time goes in v3:
time: 363 us; the launch traced here: 362 us
  waiting for transfers between devices  210 us (58%)
  starting transfers between devices  74.5 us (21%)
  matrix products  28.3 us (8%)
  other arithmetic  20.7 us (6%)
  Pallas kernels  20 us (6%)
  local copies, waits for them, and re-layouts  7.96 us (2%)
    ppermute x5, waiting for transfers between devices, hand_round(): lax.ppermute(value, 'fs', [(e * copies + c, e * copies + (c + step) % cop...  86.6 us
    all_to_all x7, waiting for transfers between devices, exchange(): lax.all_to_all(value, 'fs', split_axis=0, concat_axis=0, tiled=True, axis...  78.2 us
    all_to_all x7, starting transfers between devices, exchange(): lax.all_to_all(value, 'fs', split_axis=0, concat_axis=0, tiled=True, axis...  36.1 us
    ppermute x6, waiting for transfers between devices, along_line(): lax.ppermute(value, 'fs', [((z * inner + y) * copies + c, ((z + step) * i...  34.5 us
    ppermute x6, starting transfers between devices, along_line(): lax.ppermute(value, 'fs', [((z * inner + y) * copies + c, ((z + step) * i...  24.1 us
    pallas_call x3, Pallas kernels, place(): pl.pallas_call(functools.partial(place_kernel, moves, len(arrays)), grid_...  14.9 us
    ppermute x4, waiting for transfers between devices, across(): lax.ppermute(value, 'fs', [((z * inner + y) * copies + c, (z * inner + 1...  10.4 us
    dot_general x1, matrix products, body(): up_act = jnp.dot(piece, up_new[0], preferred_element_type=jnp.float32)  9.79 us
  transfers between devices with their start and end apart: 26, of which 12 were waited for; matrix products, arithmetic and copies ran while one was open for 13% of the time, Pallas kernels for 6%

profile of v3, /device:TPU:0, one launch (start us, length us, event | category | flops | bytes accessed | tf_op | source)
XLA Modules:
  0.0 362.1 jit_solution(4456629164923346938)
XLA Ops:
  0.6 3.2 multiply_convert_fusion.2
  3.8 7.4 %all-to-all-start = ((bf16[8,80,1024]{2,1,0:T(8,128)(2,1)}), bf16[8,80,1024]{2,1,0:T(8,128)(2,1)}, u32[]{:S(2)}, u32[]{:S(2)}) async-start(bf16[8,80,1024]{2,1,0:T(8,128)(2,1)} %multiply_convert_fusion.2), calls=%async_computation | async-start | bytes 2621440 | tf_op jit(solution)/shard_map/all_to_all | solution.py:111
  13.6 1.6 multiply_convert_fusion.4
  15.3 1.6 multiply_convert_fusion.3
  18.2 24.6 %all-to-all-done.refs_0_ = bf16[8,80,1024]{2,1,0:T(8,128)(2,1)} async-done(((bf16[8,80,1024]{2,1,0:T(8,128)(2,1)}), bf16[8,80,1024]{2,1,0:T(8,128)(2,1)}, u32[]{:S(2)}, u32[]{:S(2)}) %all-to-all-start) | async-done | bytes 1310752 | tf_op jit(solution)/shard_map/all_to_all | solution.py:111
  42.8 3.6 %all-to-all-start.1 = ((bf16[8,96,1024]{2,1,0:T(8,128)(2,1)}), bf16[8,96,1024]{2,1,0:T(8,128)(2,1)S(1)}, u32[]{:S(2)}, u32[]{:S(2)}) async-start(bf16[8,96,1024]{2,1,0:T(8,128)(2,1)} %pad_maximum_fusion), calls=%async_computation.1 | async-start | bytes 3145728 | tf_op jit(solution)/shard_map/all_to_all | solution.py:111
  46.5 3.2 multiply_convert_fusion.1
  49.7 33.9 %all-to-all-done.1.refs_2_.refs_0_ = bf16[8,96,1024]{2,1,0:T(8,128)(2,1)S(1)} async-done(((bf16[8,96,1024]{2,1,0:T(8,128)(2,1)}), bf16[8,96,1024]{2,1,0:T(8,128)(2,1)S(1)}, u32[]{:S(2)}, u32[]{:S(2)}) %all-to-all-start.1) | async-done | bytes 1572896 | tf_op jit(solution)/shard_map/all_to_all | solution.py:111
  83.6 4.3 %all-to-all-start.2 = ((bf16[8,80,1024]{2,1,0:T(8,128)(2,1)}), bf16[8,80,1024]{2,1,0:T(8,128)(2,1)}, u32[]{:S(2)}, u32[]{:S(2)}) async-start(bf16[8,80,1024]{2,1,0:T(8,128)(2,1)} %multiply_convert_fusion.1), calls=%async_computation.2 | async-start | bytes 2621440 | tf_op jit(solution)/shard_map/all_to_all | solution.py:111
  87.9 1.3 collective-permute-start
  89.2 4.6 %collective-permute-start.1 = (bf16[192,1152]{1,0:T(8,128)(2,1)}, bf16[192,1152]{1,0:T(8,128)(2,1)S(1)}, u32[]{:S(2)}, u32[]{:S(2)}) collective-permute-start(bf16[192,1152]{1,0:T(8,128)(2,1)} %get-tuple-element.57), channel_id=1, source_target_pairs={{0,8},{2,10},{4,12},{6,14},{8,16},{10,18},{12,20},{14,22},{16,24},... | collective-permute-start | bytes 1327112 | tf_op jit(solution)/shard_map/ppermute | solution.py:199
  93.8 1.9 collective-permute-start.6
  95.7 2.5 convert.4
  98.2 1.6 fusion.43
  99.8 20.3 %collective-permute-done = bf16[192,1152]{1,0:T(8,128)(2,1)S(1)} collective-permute-done((bf16[192,1152]{1,0:T(8,128)(2,1)}, bf16[192,1152]{1,0:T(8,128)(2,1)S(1)}, u32[]{:S(2)}, u32[]{:S(2)}) %collective-permute-start) | collective-permute-done | bytes 442400 | tf_op jit(solution)/shard_map/ppermute | solution.py:199
  120.2 1.3 collective-permute-start.2
  121.5 11.3 %collective-permute-start.3 = (bf16[192,1152]{1,0:T(8,128)(2,1)S(1)}, bf16[192,1152]{1,0:T(8,128)(2,1)S(1)}, u32[]{:S(2)}, u32[]{:S(2)}) collective-permute-start(bf16[192,1152]{1,0:T(8,128)(2,1)S(1)} %collective-permute-done.1), channel_id=1, source_target_pairs={{0,8},{2,10},{4,12},{6,14},{8,16},{10,18},{12,20},{14,22},{16,24},... | collective-permute-start | bytes 1327112 | tf_op jit(solution)/shard_map/ppermute | solution.py:199
  132.8 1.5 collective-permute-start.7
  134.3 6.4 %collective-permute-done.3 = bf16[192,1152]{1,0:T(8,128)(2,1)S(1)} collective-permute-done((bf16[192,1152]{1,0:T(8,128)(2,1)S(1)}, bf16[192,1152]{1,0:T(8,128)(2,1)S(1)}, u32[]{:S(2)}, u32[]{:S(2)}) %collective-permute-start.3) | collective-permute-done | bytes 442400 | tf_op jit(solution)/shard_map/ppermute | solution.py:199
  140.7 4.4 %collective-permute-start.5 = (bf16[192,1152]{1,0:T(8,128)(2,1)S(1)}, bf16[192,1152]{1,0:T(8,128)(2,1)S(1)}, u32[]{:S(2)}, u32[]{:S(2)}) collective-permute-start(bf16[192,1152]{1,0:T(8,128)(2,1)S(1)} %collective-permute-done.3), channel_id=1, source_target_pairs={{0,8},{2,10},{4,12},{6,14},{8,16},{10,18},{12,20},{14,22},{16,24},... | collective-permute-start | bytes 1327112 | tf_op jit(solution)/shard_map/ppermute | solution.py:199
  145.1 1.3 collective-permute-start.4
  146.5 2.2 collective-permute-start.8
  148.7 3.6 collective-permute-done.5
  152.3 4.2 %collective-permute-done.4 = bf16[192,1152]{1,0:T(8,128)(2,1)S(1)} collective-permute-done((bf16[192,1152]{1,0:T(8,128)(2,1)S(1)}, bf16[192,1152]{1,0:T(8,128)(2,1)S(1)}, u32[]{:S(2)}, u32[]{:S(2)}) %collective-permute-start.4) | collective-permute-done | bytes 442400 | tf_op jit(solution)/shard_map/ppermute | solution.py:199
  157.3 2.9 collective-permute-start.9
  160.2 3.6 all-to-all-start.3
  164.4 1.5 collective-permute-start.12
  165.9 10.3 %collective-permute-done.9 = bf16[192,1152]{1,0:T(8,128)(2,1)} collective-permute-done((bf16[192,1152]{1,0:T(8,128)(2,1)}, bf16[192,1152]{1,0:T(8,128)(2,1)}, u32[]{:S(2)}, u32[]{:S(2)}) %collective-permute-start.9) | collective-permute-done | bytes 442400 | tf_op jit(solution)/shard_map/ppermute | solution.py:212
  176.3 5.0 %shard_map.129 = bf16[8,96,1024]{2,1,0:T(8,128)(2,1)} custom-call(s32[9]{0:T(128)} %pad_add_fusion.1.where_ref, bf16[1,192,1152]{2,1,0:T(8,128)(2,1)} %get-tuple-element.56.refs_0_, bf16[1,192,1152]{2,1,0:T(8,128)(2,1)} %bitcast.57, bf16[1,192,1152]{2,1,0:T(8,128)(2,1)} %bitcast.58, bf16[1,192,1152]{2,1,0:T(8,128)(2,1)} %bitcast.6.refs_3_, ...), custom_call_target="tpu_custom_call" | custom-call | flops 301989888 | bytes 7077888 | tf_op jit(solution)/shard_map/pallas_call | solution.py:86
  181.3 1.5 collective-permute-start.11
  183.9 46.0 %collective-permute-done.11.refs_1_ = bf16[8,80,1024]{2,1,0:T(8,128)(2,1)} collective-permute-done((bf16[8,80,1024]{2,1,0:T(8,128)(2,1)}, bf16[8,80,1024]{2,1,0:T(8,128)(2,1)}, u32[]{:S(2)}, u32[]{:S(2)}) %collective-permute-start.11) | collective-permute-done | bytes 1310752 | tf_op jit(solution)/shard_map/ppermute | solution.py:117
  229.9 5.5 %shard_map.130 = bf16[16,128,1024]{2,1,0:T(8,128)(2,1)} custom-call(s32[16]{0:T(128)} %fusion.34.where_ref, bf16[8,80,1024]{2,1,0:T(8,128)(2,1)} %all-to-all-done.refs_0_, bf16[8,80,1024]{2,1,0:T(8,128)(2,1)} %collective-permute-done.11.refs_1_, bf16[8,96,1024]{2,1,0:T(8,128)(2,1)} %copy-done, bf16[8,96,1024]{2,1,0:T(8,128)(2,1)} %collective-permute-done.12.refs_3_.refs_1_), custom_call_target="tpu_custom_call" | custom-call | flops 23068672 | bytes 11534336 | tf_op jit(solution)/shard_map/pallas_call | solution.py:48
  235.4 5.9 %all-to-all-start.4 = ((bf16[8,64,1024]{2,1,0:T(8,128)(2,1)}), bf16[8,64,1024]{2,1,0:T(8,128)(2,1)S(1)}, u32[]{:S(2)}, u32[]{:S(2)}) async-start(bf16[8,64,1024]{2,1,0:T(8,128)(2,1)} %get-tuple-element.37), calls=%async_computation.4 | async-start | bytes 2097152 | tf_op jit(solution)/shard_map/all_to_all | solution.py:111
  241.4 9.3 %fusion.23 = f32[768,1024]{1,0:T(8,128)} fusion(bf16[2048,1024]{1,0:T(8,128)(2,1)} %bitcast.51, bf16[768,1024]{1,0:T(8,128)(2,1)} %collective-permute-done.10, bf16[768,1024]{1,0:T(8,128)(2,1)} %bitcast.60, pred[]{:T(512)S(6)} %eq.113), kind=kOutput, calls=%fused_computation.50 | convolution fusion | flops 3235381248 | bytes 10485761 | tf_op jit(solution)/shard_map/dot_general | solution.py:278
  250.6 3.4 collective-permute-done.13.refs_3_
  254.1 5.2 %shard_map.131 = bf16[16,128,1024]{2,1,0:T(8,128)(2,1)} custom-call(s32[16]{0:T(128)} %fusion.34.where_ref, bf16[8,96,1024]{2,1,0:T(8,128)(2,1)} %copy-done, bf16[8,96,1024]{2,1,0:T(8,128)(2,1)} %collective-permute-done.12.refs_3_.refs_1_, bf16[8,80,1024]{2,1,0:T(8,128)(2,1)} %all-to-all-done.2.refs_2_, bf16[8,80,1024]{2,1,0:T(8,128)(2,1)} %collective-permute-done.13.refs_3_), custom_call_target="tpu_custom_call" | custom-call | flops 23068672 | bytes 11534336 | tf_op jit(solution)/shard_map/pallas_call | solution.py:48
  259.3 9.8 %multiply_convert_fusion = bf16[768,1024]{1,0:T(8,128)(2,1)} fusion(f32[768,1024]{1,0:T(8,128)} %fusion.23, bf16[2048,1024]{1,0:T(8,128)(2,1)} %bitcast.53, bf16[768,1024]{1,0:T(8,128)(2,1)} %collective-permute-done.10, bf16[768,1024]{1,0:T(8,128)(2,1)} %bitcast.61, pred[]{:T(512)S(6)} %eq.113), kind=kOutput, calls=%fused_computation.3 | convolution fusion | flops 3240099840 | bytes 12058625 | tf_op jit(solution)/shard_map/dot_general | solution.py:279
  269.3 1.7 copy-done.12
  272.1 1.6 collective-permute-start.15
  276.3 5.6 %all-to-all-start.5 = ((bf16[8,96,512]{2,1,0:T(8,128)(2,1)}), bf16[8,96,512]{2,1,0:T(8,128)(2,1)S(1)}, u32[]{:S(2)}, u32[]{:S(2)}) async-start(bf16[8,96,512]{2,1,0:T(8,128)(2,1)} %bitcast.56), calls=%async_computation.5 | async-start | bytes 1572864 | tf_op jit(solution)/shard_map/all_to_all | solution.py:111
  282.0 16.3 %collective-permute-done.15.refs_1_ = bf16[8,64,1024]{2,1,0:T(8,128)(2,1)} collective-permute-done((bf16[8,64,1024]{2,1,0:T(8,128)(2,1)S(1)}, bf16[8,64,1024]{2,1,0:T(8,128)(2,1)}, u32[]{:S(2)}, u32[]{:S(2)}) %collective-permute-start.15) | collective-permute-done | bytes 1048608 | tf_op jit(solution)/shard_map/ppermute | solution.py:117
  299.4 20.8 %collective-permute-done.16.refs_3_ = bf16[8,64,1024]{2,1,0:T(8,128)(2,1)} collective-permute-done((bf16[8,64,1024]{2,1,0:T(8,128)(2,1)S(1)}, bf16[8,64,1024]{2,1,0:T(8,128)(2,1)}, u32[]{:S(2)}, u32[]{:S(2)}) %collective-permute-start.16) | collective-permute-done | bytes 1048608 | tf_op jit(solution)/shard_map/ppermute | solution.py:117
  321.3 1.9 convolution_convert_fusion.1
  323.5 1.3 constant_dynamic-slice_fusion
  324.8 2.4 convolution_convert_fusion
  328.3 5.6 %all-to-all-start.6 = ((bf16[8,96,512]{2,1,0:T(8,128)(2,1)}), bf16[8,96,512]{2,1,0:T(8,128)(2,1)S(1)}, u32[]{:S(2)}, u32[]{:S(2)}) async-start(bf16[8,96,512]{2,1,0:T(8,128)(2,1)} %bitcast.26), calls=%async_computation.6 | async-start | bytes 1572864 | tf_op jit(solution)/shard_map/all_to_all | solution.py:111
  335.1 19.7 %all-to-all-done.6 = bf16[8,96,512]{2,1,0:T(8,128)(2,1)S(1)} async-done(((bf16[8,96,512]{2,1,0:T(8,128)(2,1)}), bf16[8,96,512]{2,1,0:T(8,128)(2,1)S(1)}, u32[]{:S(2)}, u32[]{:S(2)}) %all-to-all-start.6) | async-done | bytes 786464 | tf_op jit(solution)/shard_map/all_to_all | solution.py:111
  356.7 4.2 %shard_map.132 = bf16[16,128,1024]{2,1,0:T(8,128)(2,1)} custom-call(s32[16]{0:T(128)} %fusion.34.where_ref, bf16[8,64,1024]{2,1,0:T(8,128)(2,1)} %copy-done.1, bf16[8,64,1024]{2,1,0:T(8,128)(2,1)} %collective-permute-done.15.refs_1_, bf16[8,64,1024]{2,1,0:T(8,128)(2,1)} %copy-done.2, bf16[8,64,1024]{2,1,0:T(8,128)(2,1)} %collective-permute-done.16.refs_3_), custom_call_target="tpu_custom_call" | custom-call | flops 16777216 | bytes 8388608 | tf_op jit(solution)/shard_map/pallas_call | solution.py:48
  (98 shorter events, 18.0 us)
Async XLA Ops:
  3.8 7.5 %copy-start.3 = (bf16[192,2048]{1,0:T(8,128)(2,1)S(1)}, bf16[192,2048]{1,0:T(8,128)(2,1)}, u32[]{:S(2)}) copy-start(bf16[192,2048]{1,0:T(8,128)(2,1)} %param.10) | copy-start | bytes 2359300
  3.8 38.9 %all-to-all-start = ((bf16[8,80,1024]{2,1,0:T(8,128)(2,1)}), bf16[8,80,1024]{2,1,0:T(8,128)(2,1)}, u32[]{:S(2)}, u32[]{:S(2)}) async-start(bf16[8,80,1024]{2,1,0:T(8,128)(2,1)} %multiply_convert_fusion.2), calls=%async_computation | async-start | bytes 2621440 | tf_op jit(solution)/shard_map/all_to_all | solution.py:111
  11.3 0.7 copy-start.6
  11.5 2.1 copy-start.7
  42.8 40.8 %all-to-all-start.1 = ((bf16[8,96,1024]{2,1,0:T(8,128)(2,1)}), bf16[8,96,1024]{2,1,0:T(8,128)(2,1)S(1)}, u32[]{:S(2)}, u32[]{:S(2)}) async-start(bf16[8,96,1024]{2,1,0:T(8,128)(2,1)} %pad_maximum_fusion), calls=%async_computation.1 | async-start | bytes 3145728 | tf_op jit(solution)/shard_map/all_to_all | solution.py:111
  83.6 80.8 %copy-start = (bf16[8,96,1024]{2,1,0:T(8,128)(2,1)}, bf16[8,96,1024]{2,1,0:T(8,128)(2,1)S(1)}, u32[]{:S(2)}) copy-start(bf16[8,96,1024]{2,1,0:T(8,128)(2,1)S(1)} %all-to-all-done.1.refs_2_.refs_0_) | copy-start | bytes 4718596
  83.6 76.6 %all-to-all-start.2 = ((bf16[8,80,1024]{2,1,0:T(8,128)(2,1)}), bf16[8,80,1024]{2,1,0:T(8,128)(2,1)}, u32[]{:S(2)}, u32[]{:S(2)}) async-start(bf16[8,80,1024]{2,1,0:T(8,128)(2,1)} %multiply_convert_fusion.1), calls=%async_computation.2 | async-start | bytes 2621440 | tf_op jit(solution)/shard_map/all_to_all | solution.py:111
  87.9 32.3 %collective-permute-start = (bf16[192,1152]{1,0:T(8,128)(2,1)}, bf16[192,1152]{1,0:T(8,128)(2,1)S(1)}, u32[]{:S(2)}, u32[]{:S(2)}) collective-permute-start(bf16[192,1152]{1,0:T(8,128)(2,1)} %get-tuple-element.57), channel_id=1, source_target_pairs={{8,0},{10,2},{12,4},{14,6},{16,8},{18,10},{20,12},{22,14},{24,16},... | collective-permute-start | bytes 1327112 | tf_op jit(solution)/shard_map/ppermute | solution.py:199
  89.2 32.3 %collective-permute-start.1 = (bf16[192,1152]{1,0:T(8,128)(2,1)}, bf16[192,1152]{1,0:T(8,128)(2,1)S(1)}, u32[]{:S(2)}, u32[]{:S(2)}) collective-permute-start(bf16[192,1152]{1,0:T(8,128)(2,1)} %get-tuple-element.57), channel_id=1, source_target_pairs={{0,8},{2,10},{4,12},{6,14},{8,16},{10,18},{12,20},{14,22},{16,24},... | collective-permute-start | bytes 1327112 | tf_op jit(solution)/shard_map/ppermute | solution.py:199
  93.8 72.2 %collective-permute-start.6 = (bf16[192,1152]{1,0:T(8,128)(2,1)}, bf16[192,1152]{1,0:T(8,128)(2,1)}, u32[]{:S(2)}, u32[]{:S(2)}) collective-permute-start(bf16[192,1152]{1,0:T(8,128)(2,1)} %get-tuple-element.57), channel_id=1, source_target_pairs={{0,4},{2,6},{4,0},{6,2},{8,12},{10,14},{12,8},{14,10},{16,20},{18,... | collective-permute-start | bytes 1327112 | tf_op jit(solution)/shard_map/ppermute | solution.py:212
  99.8 60.3 %copy-start.8 = (s32[4,4]{1,0:T(4,128)S(1)}, s32[4,4]{1,0:T(4,128)}, u32[]{:S(2)}) copy-start(s32[4,4]{1,0:T(4,128)} %constant.126.clone) | copy-start | bytes 196
  120.2 25.0 %collective-permute-start.2 = (bf16[192,1152]{1,0:T(8,128)(2,1)S(1)}, bf16[192,1152]{1,0:T(8,128)(2,1)S(1)}, u32[]{:S(2)}, u32[]{:S(2)}) collective-permute-start(bf16[192,1152]{1,0:T(8,128)(2,1)S(1)} %collective-permute-done), channel_id=1, source_target_pairs={{8,0},{10,2},{12,4},{14,6},{16,8},{18,10},{20,12},{22,14},{24,16},... | collective-permute-start | bytes 1327112 | tf_op jit(solution)/shard_map/ppermute | solution.py:199
  121.5 19.2 %collective-permute-start.3 = (bf16[192,1152]{1,0:T(8,128)(2,1)S(1)}, bf16[192,1152]{1,0:T(8,128)(2,1)S(1)}, u32[]{:S(2)}, u32[]{:S(2)}) collective-permute-start(bf16[192,1152]{1,0:T(8,128)(2,1)S(1)} %collective-permute-done.1), channel_id=1, source_target_pairs={{0,8},{2,10},{4,12},{6,14},{8,16},{10,18},{12,20},{14,22},{16,24},... | collective-permute-start | bytes 1327112 | tf_op jit(solution)/shard_map/ppermute | solution.py:199
  132.8 27.4 %copy-start.4 = (bf16[192,1152]{1,0:T(8,128)(2,1)}, bf16[192,1152]{1,0:T(8,128)(2,1)S(1)}, u32[]{:S(2)}) copy-start(bf16[192,1152]{1,0:T(8,128)(2,1)S(1)} %broadcast_select_fusion.1) | copy-start | bytes 1327108
  132.8 33.1 %collective-permute-start.7 = (bf16[192,1152]{1,0:T(8,128)(2,1)S(1)}, bf16[192,1152]{1,0:T(8,128)(2,1)}, u32[]{:S(2)}, u32[]{:S(2)}) collective-permute-start(bf16[192,1152]{1,0:T(8,128)(2,1)S(1)} %broadcast_select_fusion.1), channel_id=1, source_target_pairs={{0,4},{2,6},{4,0},{6,2},{8,12},{10,14},{12,8},{14,10},{16,20},{18,... | collective-permute-start | bytes 1327112 | tf_op jit(solution)/shard_map/ppermute | solution.py:212
  140.7 11.6 %collective-permute-start.5 = (bf16[192,1152]{1,0:T(8,128)(2,1)S(1)}, bf16[192,1152]{1,0:T(8,128)(2,1)S(1)}, u32[]{:S(2)}, u32[]{:S(2)}) collective-permute-start(bf16[192,1152]{1,0:T(8,128)(2,1)S(1)} %collective-permute-done.3), channel_id=1, source_target_pairs={{0,8},{2,10},{4,12},{6,14},{8,16},{10,18},{12,20},{14,22},{16,24},... | collective-permute-start | bytes 1327112 | tf_op jit(solution)/shard_map/ppermute | solution.py:199
  145.1 11.3 %collective-permute-start.4 = (bf16[192,1152]{1,0:T(8,128)(2,1)S(1)}, bf16[192,1152]{1,0:T(8,128)(2,1)S(1)}, u32[]{:S(2)}, u32[]{:S(2)}) collective-permute-start(bf16[192,1152]{1,0:T(8,128)(2,1)S(1)} %collective-permute-done.2), channel_id=1, source_target_pairs={{8,0},{10,2},{12,4},{14,6},{16,8},{18,10},{20,12},{22,14},{24,16},... | collective-permute-start | bytes 1327112 | tf_op jit(solution)/shard_map/ppermute | solution.py:199
  146.5 29.8 %copy-start.5 = (bf16[192,1152]{1,0:T(8,128)(2,1)}, bf16[192,1152]{1,0:T(8,128)(2,1)S(1)}, u32[]{:S(2)}) copy-start(bf16[192,1152]{1,0:T(8,128)(2,1)S(1)} %broadcast_select_fusion) | copy-start | bytes 1327108
  146.5 19.4 %collective-permute-start.8 = (bf16[192,1152]{1,0:T(8,128)(2,1)S(1)}, bf16[192,1152]{1,0:T(8,128)(2,1)}, u32[]{:S(2)}, u32[]{:S(2)}) collective-permute-start(bf16[192,1152]{1,0:T(8,128)(2,1)S(1)} %broadcast_select_fusion), channel_id=1, source_target_pairs={{0,4},{2,6},{4,0},{6,2},{8,12},{10,14},{12,8},{14,10},{16,20},{18,... | collective-permute-start | bytes 1327112 | tf_op jit(solution)/shard_map/ppermute | solution.py:212
  157.3 19.0 %collective-permute-start.9 = (bf16[192,1152]{1,0:T(8,128)(2,1)}, bf16[192,1152]{1,0:T(8,128)(2,1)}, u32[]{:S(2)}, u32[]{:S(2)}) collective-permute-start(bf16[192,1152]{1,0:T(8,128)(2,1)} %select_select_fusion), channel_id=1, source_target_pairs={{0,4},{2,6},{4,0},{6,2},{8,12},{10,14},{12,8},{14,10},{16,20},{18,... | collective-permute-start | bytes 1327112 | tf_op jit(solution)/shard_map/ppermute | solution.py:212
  160.2 75.2 %all-to-all-start.3 = ((bf16[8,64,1024]{2,1,0:T(8,128)(2,1)}), bf16[8,64,1024]{2,1,0:T(8,128)(2,1)S(1)}, u32[]{:S(2)}, u32[]{:S(2)}) async-start(bf16[8,64,1024]{2,1,0:T(8,128)(2,1)} %get-tuple-element.35), calls=%async_computation.3 | async-start | bytes 2097152 | tf_op jit(solution)/shard_map/all_to_all | solution.py:111
  164.4 65.5 %collective-permute-start.12 = (bf16[8,96,1024]{2,1,0:T(8,128)(2,1)S(1)}, bf16[8,96,1024]{2,1,0:T(8,128)(2,1)}, u32[]{:S(2)}, u32[]{:S(2)}) collective-permute-start(bf16[8,96,1024]{2,1,0:T(8,128)(2,1)S(1)} %all-to-all-done.1.refs_2_.refs_0_), channel_id=1, source_target_pairs={{0,2},{2,0},{4,6},{6,4},{8,10},{10,8},{12,14},{14,12},{16,18},{18,... | collective-permute-start | bytes 4718600 | tf_op jit(solution)/shard_map/ppermute | solution.py:117
  176.3 7.1 %copy-start.10 = (s32[16]{0:T(128)S(1)}, s32[16]{0:T(128)}, u32[]{:S(2)}) copy-start(s32[16]{0:T(128)} %constant.128.clone) | copy-start | bytes 196
  176.3 7.1 %copy-start.11 = (s32[16]{0:T(128)S(1)}, s32[16]{0:T(128)}, u32[]{:S(2)}) copy-start(s32[16]{0:T(128)} %constant.131) | copy-start | bytes 196
  181.3 60.0 %collective-permute-start.10 = (bf16[768,1024]{1,0:T(8,128)(2,1)}, bf16[768,1024]{1,0:T(8,128)(2,1)}, u32[]{:S(2)}, u32[]{:S(2)}) collective-permute-start(bf16[768,1024]{1,0:T(8,128)(2,1)} %bitcast.59), channel_id=1, source_target_pairs={{0,1},{1,0},{2,3},{3,2},{4,5},{5,4},{6,7},{7,6},{8,9},{9,8},{10,11... | collective-permute-start | bytes 4718600 | tf_op jit(solution)/shard_map/ppermute | solution.py:130
  181.3 48.6 %collective-permute-start.11 = (bf16[8,80,1024]{2,1,0:T(8,128)(2,1)}, bf16[8,80,1024]{2,1,0:T(8,128)(2,1)}, u32[]{:S(2)}, u32[]{:S(2)}) collective-permute-start(bf16[8,80,1024]{2,1,0:T(8,128)(2,1)} %all-to-all-done.refs_0_), channel_id=1, source_target_pairs={{0,2},{2,0},{4,6},{6,4},{8,10},{10,8},{12,14},{14,12},{16,18},{18,... | collective-permute-start | bytes 3932168 | tf_op jit(solution)/shard_map/ppermute | solution.py:117
  182.8 71.2 %collective-permute-start.13 = (bf16[8,80,1024]{2,1,0:T(8,128)(2,1)}, bf16[8,80,1024]{2,1,0:T(8,128)(2,1)}, u32[]{:S(2)}, u32[]{:S(2)}) collective-permute-start(bf16[8,80,1024]{2,1,0:T(8,128)(2,1)} %all-to-all-done.2.refs_2_), channel_id=1, source_target_pairs={{0,2},{2,0},{4,6},{6,4},{8,10},{10,8},{12,14},{14,12},{16,18},{18,... | collective-permute-start | bytes 3932168 | tf_op jit(solution)/shard_map/ppermute | solution.py:117
  235.4 36.7 %copy-start.1 = (bf16[8,64,1024]{2,1,0:T(8,128)(2,1)}, bf16[8,64,1024]{2,1,0:T(8,128)(2,1)S(1)}, u32[]{:S(2)}) copy-start(bf16[8,64,1024]{2,1,0:T(8,128)(2,1)S(1)} %all-to-all-done.3.refs_0_) | copy-start | bytes 3145732
  235.4 33.8 %all-to-all-start.4 = ((bf16[8,64,1024]{2,1,0:T(8,128)(2,1)}), bf16[8,64,1024]{2,1,0:T(8,128)(2,1)S(1)}, u32[]{:S(2)}, u32[]{:S(2)}) async-start(bf16[8,64,1024]{2,1,0:T(8,128)(2,1)} %get-tuple-element.37), calls=%async_computation.4 | async-start | bytes 2097152 | tf_op jit(solution)/shard_map/all_to_all | solution.py:111
  269.2 4.5 %copy-start.2 = (bf16[8,64,1024]{2,1,0:T(8,128)(2,1)}, bf16[8,64,1024]{2,1,0:T(8,128)(2,1)S(1)}, u32[]{:S(2)}) copy-start(bf16[8,64,1024]{2,1,0:T(8,128)(2,1)S(1)} %all-to-all-done.4.refs_2_) | copy-start | bytes 3145732
  269.2 1.8 copy-start.12
  272.0 3.2 collective-permute-start.14
  272.1 26.2 %collective-permute-start.15 = (bf16[8,64,1024]{2,1,0:T(8,128)(2,1)S(1)}, bf16[8,64,1024]{2,1,0:T(8,128)(2,1)}, u32[]{:S(2)}, u32[]{:S(2)}) collective-permute-start(bf16[8,64,1024]{2,1,0:T(8,128)(2,1)S(1)} %all-to-all-done.3.refs_0_), channel_id=1, source_target_pairs={{0,2},{2,0},{4,6},{6,4},{8,10},{10,8},{12,14},{14,12},{16,18},{18,... | collective-permute-start | bytes 3145736 | tf_op jit(solution)/shard_map/ppermute | solution.py:117
  273.6 46.6 %collective-permute-start.16 = (bf16[8,64,1024]{2,1,0:T(8,128)(2,1)S(1)}, bf16[8,64,1024]{2,1,0:T(8,128)(2,1)}, u32[]{:S(2)}, u32[]{:S(2)}) collective-permute-start(bf16[8,64,1024]{2,1,0:T(8,128)(2,1)S(1)} %all-to-all-done.4.refs_2_), channel_id=1, source_target_pairs={{0,2},{2,0},{4,6},{6,4},{8,10},{10,8},{12,14},{14,12},{16,18},{18,... | collective-permute-start | bytes 3145736 | tf_op jit(solution)/shard_map/ppermute | solution.py:117
  276.3 52.0 %all-to-all-start.5 = ((bf16[8,96,512]{2,1,0:T(8,128)(2,1)}), bf16[8,96,512]{2,1,0:T(8,128)(2,1)S(1)}, u32[]{:S(2)}, u32[]{:S(2)}) async-start(bf16[8,96,512]{2,1,0:T(8,128)(2,1)} %bitcast.56), calls=%async_computation.5 | async-start | bytes 1572864 | tf_op jit(solution)/shard_map/all_to_all | solution.py:111
  282.0 39.3 %copy-start.13 = (bf16[768,1024]{1,0:T(8,128)(2,1)S(1)}, bf16[768,1024]{1,0:T(8,128)(2,1)}, u32[]{:S(2)}) copy-start(bf16[768,1024]{1,0:T(8,128)(2,1)} %multiply_convert_fusion) | copy-start | bytes 4718596
  323.2 4.0 %collective-permute-start.17 = (bf16[768,512]{1,0:T(8,128)(2,1)}, bf16[768,512]{1,0:T(8,128)(2,1)S(1)}, u32[]{:S(2)}, u32[]{:S(2)}) collective-permute-start(bf16[768,512]{1,0:T(8,128)(2,1)} %convolution_convert_fusion.1), channel_id=1, source_target_pairs={{0,1},{1,0},{2,3},{3,2},{4,5},{5,4},{6,7},{7,6},{8,9},{9,8},{10,11... | collective-permute-start | bytes 2359304 | tf_op jit(solution)/shard_map/ppermute | solution.py:130
  327.2 7.1 %copy-start.9 = (f32[192,2]{0,1:T(2,128)S(1)}, f32[192,2]{0,1:T(2,128)}, u32[]{:S(2)}) copy-start(f32[192,2]{0,1:T(2,128)} %param.12) | copy-start | bytes 4612
  328.3 26.5 %all-to-all-start.6 = ((bf16[8,96,512]{2,1,0:T(8,128)(2,1)}), bf16[8,96,512]{2,1,0:T(8,128)(2,1)S(1)}, u32[]{:S(2)}, u32[]{:S(2)}) async-start(bf16[8,96,512]{2,1,0:T(8,128)(2,1)} %bitcast.26), calls=%async_computation.6 | async-start | bytes 1572864 | tf_op jit(solution)/shard_map/all_to_all | solution.py:111
  356.7 4.3 %collective-permute-start.18 = (bf16[192,1024]{1,0:T(8,128)(2,1)S(1)}, bf16[192,1024]{1,0:T(8,128)(2,1)S(1)}, u32[]{:S(2)}, u32[]{:S(2)}) collective-permute-start(bf16[192,1024]{1,0:T(8,128)(2,1)S(1)} %fusion.2), channel_id=1, source_target_pairs={{0,1},{1,0},{2,3},{3,2},{4,5},{5,4},{6,7},{7,6},{8,9},{9,8},{10,11... | collective-permute-start | bytes 1179656 | tf_op jit(solution)/shard_map/ppermute | solution.py:130

commit v4 on v3

--- a/solution.py
+++ b/solution.py
@@ -132,14 +132,13 @@
     def join_cols(part):
         if tp_count == 2:
             other = other_core(part)
-            return jnp.where(
-                tp_index == 0,
-                jnp.concatenate([part, other], axis=1),
-                jnp.concatenate([other, part], axis=1),
+            whole = jnp.concatenate([part, part], axis=1)
+            return lax.dynamic_update_slice_in_dim(
+                whole, other, (1 - tp_index) * part.shape[1], axis=1
             )
         return lax.all_gather(part, "tp", axis=1, tiled=True)
 
-    cuts = [2 * depth * k // 16 // 16 * 16 for k in (0, 5, 11, 16)]
+    cuts = [2 * depth * k // 16 // 16 * 16 for k in (0, 7, 12, 16)]
     spans = list(zip(cuts[:-1], cuts[1:]))
     sources = [gate_weight, up_weight]
 
@@ -251,7 +250,7 @@
     where = jnp.concatenate(order + [expert[None]]).astype(jnp.int32)
     piece_cols = pick_rows(arrays, layout, where, share_width)
     piece_cols = piece_cols.reshape(experts * CAP, share_width)
-    piece = join_cols(piece_cols)
+    piece = after(join_cols(piece_cols))
 
     spots = (block_expert * copies + (lane - block_copy) % copies).astype(jnp.int32)
     shape = (fs_count, depth, cols)

time: 363 us -> 343 us (0.945)
  waiting for transfers between devices: 210 us -> 172 us
  starting transfers between devices: 74.5 us -> 91.9 us
  local copies, waits for them, and re-layouts: 7.96 us -> 12.9 us
  matrix products: 28.3 us -> 23.9 us
    all_to_all x7, waiting for transfers between devices: 78.2 us -> 56 us  [exchange(): lax.all_to_all(value, 'fs', split_axis=0, concat_axis=0, tiled=True, axis...]
    all_to_all x7, starting transfers between devices: 36.1 us -> 48.1 us  [exchange(): lax.all_to_all(value, 'fs', split_axis=0, concat_axis=0, tiled=True, axis...]
    ppermute x4, waiting for transfers between devices: 10.4 us -> 0.01 us  [across(): lax.ppermute(value, 'fs', [((z * inner + y) * copies + c, (z * inner + 1...]
    ppermute x5, waiting for transfers between devices: 86.6 us -> 81.3 us  [hand_round(): lax.ppermute(value, 'fs', [(e * copies + c, e * copies + (c + step) % cop...]
    concatenate x0 -> x3, other arithmetic: none -> 4.98 us  [the longest x2 4 us: join_cols(): whole = jnp.concatenate([part, part], axis=1)]
    ppermute x6, starting transfers between devices: 24.1 us -> 28.3 us  [along_line(): lax.ppermute(value, 'fs', [((z * inner + y) * copies + c, ((z + step) * i...]
    convert_element_type x4 -> x3, other arithmetic: 9.66 us -> 6.65 us  [fold(): (gain[None, a:a + size, None] * sources[n][:, a:a + size]).astype(jnp.bfl...]
  transfers between devices with their start and end apart: 26 -> 26, of which waited for: 12 -> 9; matrix products, arithmetic and copies ran while one was open for 13% -> 14% of each run, Pallas kernels for 6% -> 6%
where the time goes in v4:
time: 343 us; the launch traced here: 342 us
  waiting for transfers between devices  172 us (50%)
  starting transfers between devices  91.9 us (27%)
  matrix products  23.9 us (7%)
  other arithmetic  21.4 us (6%)
  Pallas kernels  19.1 us (6%)
  local copies, waits for them, and re-layouts  12.9 us (4%)
    ppermute x5, waiting for transfers between devices, hand_round(): lax.ppermute(value, 'fs', [(e * copies + c, e * copies + (c + step) % cop...  81.3 us
    all_to_all x7, waiting for transfers between devices, exchange(): lax.all_to_all(value, 'fs', split_axis=0, concat_axis=0, tiled=True, axis...  56 us
    all_to_all x7, starting transfers between devices, exchange(): lax.all_to_all(value, 'fs', split_axis=0, concat_axis=0, tiled=True, axis...  48.1 us
    ppermute x6, waiting for transfers between devices, along_line(): lax.ppermute(value, 'fs', [((z * inner + y) * copies + c, ((z + step) * i...  34.6 us
    ppermute x6, starting transfers between devices, along_line(): lax.ppermute(value, 'fs', [((z * inner + y) * copies + c, ((z + step) * i...  28.3 us
    pallas_call x3, Pallas kernels, place(): pl.pallas_call(functools.partial(place_kernel, moves, len(arrays)), grid_...  14 us
    ppermute x4, starting transfers between devices, across(): lax.ppermute(value, 'fs', [((z * inner + y) * copies + c, (z * inner + 1...  9.52 us
    dot_general x1, matrix products, body(): up_act = jnp.dot(piece, up_new[0], preferred_element_type=jnp.float32)  8.83 us
  transfers between devices with their start and end apart: 26, of which 9 were waited for; matrix products, arithmetic and copies ran while one was open for 14% of the time, Pallas kernels for 6%

profile of v4, /device:TPU:0, one launch (start us, length us, event | category | flops | bytes accessed | tf_op | source)
XLA Modules:
  0.0 342.4 jit_solution(10798926893245178341)
XLA Ops:
  0.6 3.9 %multiply_convert_fusion = bf16[8,112,1024]{2,1,0:T(8,128)(2,1)} fusion(f32[8,128,1024]{2,1,0:T(8,128)} %param.14, f32[112]{0:T(128)} %bitcast.75), kind=kLoop, calls=%fused_computation.2 | loop fusion | flops 1835008 | bytes 5505472 | tf_op jit(solution)/shard_map/convert_element_type | solution.py:156
  4.5 7.4 %all-to-all-start = ((bf16[8,112,1024]{2,1,0:T(8,128)(2,1)}), bf16[8,112,1024]{2,1,0:T(8,128)(2,1)}, u32[]{:S(2)}, u32[]{:S(2)}) async-start(bf16[8,112,1024]{2,1,0:T(8,128)(2,1)} %multiply_convert_fusion), calls=%async_computation | async-start | bytes 3670016 | tf_op jit(solution)/shard_map/all_to_all | solution.py:111
  14.3 1.1 multiply_convert_fusion.4
  15.4 1.6 multiply_convert_fusion.2
  17.1 1.2 pad_maximum_fusion.1
  18.2 36.4 %all-to-all-done.refs_0_ = bf16[8,112,1024]{2,1,0:T(8,128)(2,1)} async-done(((bf16[8,112,1024]{2,1,0:T(8,128)(2,1)}), bf16[8,112,1024]{2,1,0:T(8,128)(2,1)}, u32[]{:S(2)}, u32[]{:S(2)}) %all-to-all-start) | async-done | bytes 1835040 | tf_op jit(solution)/shard_map/all_to_all | solution.py:111
  54.7 3.6 %all-to-all-start.1 = ((bf16[8,80,1024]{2,1,0:T(8,128)(2,1)}), bf16[8,80,1024]{2,1,0:T(8,128)(2,1)S(1)}, u32[]{:S(2)}, u32[]{:S(2)}) async-start(bf16[8,80,1024]{2,1,0:T(8,128)(2,1)} %pad_maximum_fusion.1), calls=%async_computation.1 | async-start | bytes 2621440 | tf_op jit(solution)/shard_map/all_to_all | solution.py:111
  58.3 1.3 collective-permute-start
  59.6 4.6 %collective-permute-start.1 = (bf16[192,1152]{1,0:T(8,128)(2,1)}, bf16[192,1152]{1,0:T(8,128)(2,1)S(1)}, u32[]{:S(2)}, u32[]{:S(2)}) collective-permute-start(bf16[192,1152]{1,0:T(8,128)(2,1)} %get-tuple-element.58), channel_id=1, source_target_pairs={{0,8},{2,10},{4,12},{6,14},{8,16},{10,18},{12,20},{14,22},{16,24},... | collective-permute-start | bytes 1327112 | tf_op jit(solution)/shard_map/ppermute | solution.py:198
  64.2 2.1 collective-permute-start.6
  66.3 2.5 convert.4
  68.8 1.6 fusion.39
  70.4 21.0 %collective-permute-done = bf16[192,1152]{1,0:T(8,128)(2,1)S(1)} collective-permute-done((bf16[192,1152]{1,0:T(8,128)(2,1)}, bf16[192,1152]{1,0:T(8,128)(2,1)S(1)}, u32[]{:S(2)}, u32[]{:S(2)}) %collective-permute-start) | collective-permute-done | bytes 442400 | tf_op jit(solution)/shard_map/ppermute | solution.py:198
  91.4 1.3 collective-permute-start.2
  92.7 11.8 %collective-permute-start.3 = (bf16[192,1152]{1,0:T(8,128)(2,1)S(1)}, bf16[192,1152]{1,0:T(8,128)(2,1)}, u32[]{:S(2)}, u32[]{:S(2)}) collective-permute-start(bf16[192,1152]{1,0:T(8,128)(2,1)S(1)} %collective-permute-done.1), channel_id=1, source_target_pairs={{0,8},{2,10},{4,12},{6,14},{8,16},{10,18},{12,20},{14,22},{16,24},... | collective-permute-start | bytes 1327112 | tf_op jit(solution)/shard_map/ppermute | solution.py:198
  104.6 4.2 %all-to-all-start.2 = ((bf16[8,64,1024]{2,1,0:T(8,128)(2,1)}), bf16[8,64,1024]{2,1,0:T(8,128)(2,1)}, u32[]{:S(2)}, u32[]{:S(2)}) async-start(bf16[8,64,1024]{2,1,0:T(8,128)(2,1)} %get-tuple-element.33), calls=%async_computation.2 | async-start | bytes 2097152 | tf_op jit(solution)/shard_map/all_to_all | solution.py:111
  108.9 1.9 collective-permute-start.7
  110.9 3.5 %collective-permute-done.3 = bf16[192,1152]{1,0:T(8,128)(2,1)} collective-permute-done((bf16[192,1152]{1,0:T(8,128)(2,1)S(1)}, bf16[192,1152]{1,0:T(8,128)(2,1)}, u32[]{:S(2)}, u32[]{:S(2)}) %collective-permute-start.3) | collective-permute-done | bytes 442400 | tf_op jit(solution)/shard_map/ppermute | solution.py:198
  114.4 8.0 %collective-permute-start.5 = (bf16[192,1152]{1,0:T(8,128)(2,1)}, bf16[192,1152]{1,0:T(8,128)(2,1)S(1)}, u32[]{:S(2)}, u32[]{:S(2)}) collective-permute-start(bf16[192,1152]{1,0:T(8,128)(2,1)} %collective-permute-done.3), channel_id=1, source_target_pairs={{0,8},{2,10},{4,12},{6,14},{8,16},{10,18},{12,20},{14,22},{16,24},... | collective-permute-start | bytes 1327112 | tf_op jit(solution)/shard_map/ppermute | solution.py:198
  122.4 1.3 collective-permute-start.4
  124.8 3.9 %collective-permute-start.8 = (bf16[192,1152]{1,0:T(8,128)(2,1)S(1)}, bf16[192,1152]{1,0:T(8,128)(2,1)}, u32[]{:S(2)}, u32[]{:S(2)}) collective-permute-start(bf16[192,1152]{1,0:T(8,128)(2,1)S(1)} %broadcast_select_fusion), channel_id=1, source_target_pairs={{0,4},{2,6},{4,0},{6,2},{8,12},{10,14},{12,8},{14,10},{16,20},{18,... | collective-permute-start | bytes 1327112 | tf_op jit(solution)/shard_map/ppermute | solution.py:211
  128.7 10.1 %collective-permute-done.5 = bf16[192,1152]{1,0:T(8,128)(2,1)S(1)} collective-permute-done((bf16[192,1152]{1,0:T(8,128)(2,1)}, bf16[192,1152]{1,0:T(8,128)(2,1)S(1)}, u32[]{:S(2)}, u32[]{:S(2)}) %collective-permute-start.5) | collective-permute-done | bytes 442400 | tf_op jit(solution)/shard_map/ppermute | solution.py:198
  139.7 1.6 collective-permute-start.9
  141.3 1.5 collective-permute-start.11
  142.9 10.4 %all-to-all-start.3 = ((bf16[8,64,1024]{2,1,0:T(8,128)(2,1)}), bf16[8,64,1024]{2,1,0:T(8,128)(2,1)S(1)}, u32[]{:S(2)}, u32[]{:S(2)}) async-start(bf16[8,64,1024]{2,1,0:T(8,128)(2,1)} %get-tuple-element.35), calls=%async_computation.3 | async-start | bytes 2097152 | tf_op jit(solution)/shard_map/all_to_all | solution.py:111
  153.9 5.0 %shard_map.129 = bf16[8,96,1024]{2,1,0:T(8,128)(2,1)} custom-call(s32[9]{0:T(128)} %pad_add_fusion.1.where_ref, bf16[1,192,1152]{2,1,0:T(8,128)(2,1)} %get-tuple-element.59.refs_0_, bf16[1,192,1152]{2,1,0:T(8,128)(2,1)} %bitcast.61, bf16[1,192,1152]{2,1,0:T(8,128)(2,1)} %bitcast.62, bf16[1,192,1152]{2,1,0:T(8,128)(2,1)} %bitcast.6.refs_3_, ...), custom_call_target="tpu_custom_call" | custom-call | flops 301989888 | bytes 7077888 | tf_op jit(solution)/shard_map/pallas_call | solution.py:86
  160.1 1.5 collective-permute-start.13
  161.6 3.9 %pad_maximum_fusion = bf16[768,2048]{1,0:T(8,128)(2,1)} fusion(bf16[768,1024]{1,0:T(8,128)(2,1)} %bitcast.54), kind=kLoop, calls=%fused_computation.3 | loop fusion | flops 6291456 | bytes 4718592 | tf_op jit(solution)/shard_map/concatenate | solution.py:135
  165.5 2.7 constant_dynamic-update-slice_fusion.1
  168.2 16.4 %collective-permute-done.11.refs_1_ = bf16[8,112,1024]{2,1,0:T(8,128)(2,1)} collective-permute-done((bf16[8,112,1024]{2,1,0:T(8,128)(2,1)}, bf16[8,112,1024]{2,1,0:T(8,128)(2,1)}, u32[]{:S(2)}, u32[]{:S(2)}) %collective-permute-start.11) | collective-permute-done | bytes 1835040 | tf_op jit(solution)/shard_map/ppermute | solution.py:117
  184.6 28.1 %collective-permute-done.12.refs_3_.refs_1_ = bf16[8,80,1024]{2,1,0:T(8,128)(2,1)} collective-permute-done((bf16[8,80,1024]{2,1,0:T(8,128)(2,1)S(1)}, bf16[8,80,1024]{2,1,0:T(8,128)(2,1)}, u32[]{:S(2)}, u32[]{:S(2)}) %collective-permute-start.12) | collective-permute-done | bytes 1310752 | tf_op jit(solution)/shard_map/ppermute | solution.py:117
  212.7 5.4 %shard_map.130 = bf16[16,128,1024]{2,1,0:T(8,128)(2,1)} custom-call(s32[16]{0:T(128)} %fusion.32.where_ref, bf16[8,112,1024]{2,1,0:T(8,128)(2,1)} %all-to-all-done.refs_0_, bf16[8,112,1024]{2,1,0:T(8,128)(2,1)} %collective-permute-done.11.refs_1_, bf16[8,80,1024]{2,1,0:T(8,128)(2,1)} %copy-done, bf16[8,80,1024]{2,1,0:T(8,128)(2,1)} %collective-permute-done.12.refs_3_.refs_1_), custom_call_target="tpu_custom_call" | custom-call | flops 25165824 | bytes 12582912 | tf_op jit(solution)/shard_map/pallas_call | solution.py:48
  218.1 10.4 %all-to-all-start.4 = ((bf16[8,64,1024]{2,1,0:T(8,128)(2,1)}), bf16[8,64,1024]{2,1,0:T(8,128)(2,1)S(1)}, u32[]{:S(2)}, u32[]{:S(2)}) async-start(bf16[8,64,1024]{2,1,0:T(8,128)(2,1)} %get-tuple-element.37), calls=%async_computation.4 | async-start | bytes 2097152 | tf_op jit(solution)/shard_map/all_to_all | solution.py:111
  228.5 8.2 %fusion.43 = f32[768,1024]{1,0:T(8,128)} fusion(bf16[768,2048]{1,0:T(8,128)(2,1)} %constant_dynamic-update-slice_fusion.1, bf16[2048,1024]{1,0:T(8,128)(2,1)} %bitcast.55), kind=kOutput, calls=%fused_computation.112 | convolution fusion | flops 3221225472 | bytes 10485760 | tf_op jit(solution)/shard_map/dot_general | solution.py:277
  236.7 4.5 %shard_map.131 = bf16[16,128,1024]{2,1,0:T(8,128)(2,1)} custom-call(s32[16]{0:T(128)} %fusion.32.where_ref, bf16[8,80,1024]{2,1,0:T(8,128)(2,1)} %copy-done, bf16[8,80,1024]{2,1,0:T(8,128)(2,1)} %collective-permute-done.12.refs_3_.refs_1_, bf16[8,64,1024]{2,1,0:T(8,128)(2,1)} %all-to-all-done.2.refs_2_, bf16[8,64,1024]{2,1,0:T(8,128)(2,1)} %collective-permute-done.13.refs_3_), custom_call_target="tpu_custom_call" | custom-call | flops 18874368 | bytes 9437184 | tf_op jit(solution)/shard_map/pallas_call | solution.py:48
  241.2 8.8 %multiply_convert_fusion.1 = bf16[768,1024]{1,0:T(8,128)(2,1)} fusion(f32[768,1024]{1,0:T(8,128)} %fusion.43, bf16[768,2048]{1,0:T(8,128)(2,1)} %constant_dynamic-update-slice_fusion.1, bf16[2048,1024]{1,0:T(8,128)(2,1)} %bitcast.57), kind=kOutput, calls=%fused_computation.4 | convolution fusion | flops 3225944064 | bytes 12058624 | tf_op jit(solution)/shard_map/dot_general | solution.py:278
  251.0 1.3 copy-done.8
  253.9 1.6 collective-permute-start.15
  257.1 1.1 add_convert_fusion.1
  258.2 6.0 %all-to-all-start.5 = ((bf16[8,96,512]{2,1,0:T(8,128)(2,1)}), bf16[8,96,512]{2,1,0:T(8,128)(2,1)S(1)}, u32[]{:S(2)}, u32[]{:S(2)}) async-start(bf16[8,96,512]{2,1,0:T(8,128)(2,1)} %bitcast.60), calls=%async_computation.5 | async-start | bytes 1572864 | tf_op jit(solution)/shard_map/all_to_all | solution.py:111
  264.2 16.0 %collective-permute-done.15.refs_1_ = bf16[8,64,1024]{2,1,0:T(8,128)(2,1)} collective-permute-done((bf16[8,64,1024]{2,1,0:T(8,128)(2,1)S(1)}, bf16[8,64,1024]{2,1,0:T(8,128)(2,1)}, u32[]{:S(2)}, u32[]{:S(2)}) %collective-permute-start.15) | collective-permute-done | bytes 1048608 | tf_op jit(solution)/shard_map/ppermute | solution.py:117
  281.2 20.8 %collective-permute-done.16.refs_3_ = bf16[8,64,1024]{2,1,0:T(8,128)(2,1)} collective-permute-done((bf16[8,64,1024]{2,1,0:T(8,128)(2,1)S(1)}, bf16[8,64,1024]{2,1,0:T(8,128)(2,1)}, u32[]{:S(2)}, u32[]{:S(2)}) %collective-permute-start.16) | collective-permute-done | bytes 1048608 | tf_op jit(solution)/shard_map/ppermute | solution.py:117
  304.6 1.4 constant_dynamic-slice_fusion
  307.3 1.1 add_convert_fusion
  308.4 6.0 %all-to-all-start.6 = ((bf16[8,96,512]{2,1,0:T(8,128)(2,1)}), bf16[8,96,512]{2,1,0:T(8,128)(2,1)S(1)}, u32[]{:S(2)}, u32[]{:S(2)}) async-start(bf16[8,96,512]{2,1,0:T(8,128)(2,1)} %bitcast.26), calls=%async_computation.6 | async-start | bytes 1572864 | tf_op jit(solution)/shard_map/all_to_all | solution.py:111
  315.6 19.6 %all-to-all-done.6 = bf16[8,96,512]{2,1,0:T(8,128)(2,1)S(1)} async-done(((bf16[8,96,512]{2,1,0:T(8,128)(2,1)}), bf16[8,96,512]{2,1,0:T(8,128)(2,1)S(1)}, u32[]{:S(2)}, u32[]{:S(2)}) %all-to-all-start.6) | async-done | bytes 786464 | tf_op jit(solution)/shard_map/all_to_all | solution.py:111
  335.9 1.1 fusion.2
  337.1 4.2 %shard_map.132 = bf16[16,128,1024]{2,1,0:T(8,128)(2,1)} custom-call(s32[16]{0:T(128)} %fusion.32.where_ref, bf16[8,64,1024]{2,1,0:T(8,128)(2,1)} %copy-done.1, bf16[8,64,1024]{2,1,0:T(8,128)(2,1)} %collective-permute-done.15.refs_1_, bf16[8,64,1024]{2,1,0:T(8,128)(2,1)} %copy-done.2, bf16[8,64,1024]{2,1,0:T(8,128)(2,1)} %collective-permute-done.16.refs_3_), custom_call_target="tpu_custom_call" | custom-call | flops 16777216 | bytes 8388608 | tf_op jit(solution)/shard_map/pallas_call | solution.py:48
  (108 shorter events, 18.0 us)
Async XLA Ops:
  4.5 7.4 %copy-start.9 = (s32[192,2]{0,1:T(2,128)S(1)}, s32[192,2]{0,1:T(2,128)}, u32[]{:S(2)}) copy-start(s32[192,2]{0,1:T(2,128)} %param.11) | copy-start | bytes 4612
  4.5 7.6 %copy-start.4 = (bf16[192,2048]{1,0:T(8,128)(2,1)S(1)}, bf16[192,2048]{1,0:T(8,128)(2,1)}, u32[]{:S(2)}) copy-start(bf16[192,2048]{1,0:T(8,128)(2,1)} %param.10) | copy-start | bytes 2359300
  4.5 50.2 %all-to-all-start = ((bf16[8,112,1024]{2,1,0:T(8,128)(2,1)}), bf16[8,112,1024]{2,1,0:T(8,128)(2,1)}, u32[]{:S(2)}, u32[]{:S(2)}) async-start(bf16[8,112,1024]{2,1,0:T(8,128)(2,1)} %multiply_convert_fusion), calls=%async_computation | async-start | bytes 3670016 | tf_op jit(solution)/shard_map/all_to_all | solution.py:111
  12.3 1.8 copy-start.10
  12.3 3.1 copy-start.3
  54.7 49.9 %all-to-all-start.1 = ((bf16[8,80,1024]{2,1,0:T(8,128)(2,1)}), bf16[8,80,1024]{2,1,0:T(8,128)(2,1)S(1)}, u32[]{:S(2)}, u32[]{:S(2)}) async-start(bf16[8,80,1024]{2,1,0:T(8,128)(2,1)} %pad_maximum_fusion.1), calls=%async_computation.1 | async-start | bytes 2621440 | tf_op jit(solution)/shard_map/all_to_all | solution.py:111
  58.3 33.1 %collective-permute-start = (bf16[192,1152]{1,0:T(8,128)(2,1)}, bf16[192,1152]{1,0:T(8,128)(2,1)S(1)}, u32[]{:S(2)}, u32[]{:S(2)}) collective-permute-start(bf16[192,1152]{1,0:T(8,128)(2,1)} %get-tuple-element.58), channel_id=1, source_target_pairs={{8,0},{10,2},{12,4},{14,6},{16,8},{18,10},{20,12},{22,14},{24,16},... | collective-permute-start | bytes 1327112 | tf_op jit(solution)/shard_map/ppermute | solution.py:198
  59.6 33.1 %collective-permute-start.1 = (bf16[192,1152]{1,0:T(8,128)(2,1)}, bf16[192,1152]{1,0:T(8,128)(2,1)S(1)}, u32[]{:S(2)}, u32[]{:S(2)}) collective-permute-start(bf16[192,1152]{1,0:T(8,128)(2,1)} %get-tuple-element.58), channel_id=1, source_target_pairs={{0,8},{2,10},{4,12},{6,14},{8,16},{10,18},{12,20},{14,22},{16,24},... | collective-permute-start | bytes 1327112 | tf_op jit(solution)/shard_map/ppermute | solution.py:198
  64.2 89.7 %collective-permute-start.6 = (bf16[192,1152]{1,0:T(8,128)(2,1)}, bf16[192,1152]{1,0:T(8,128)(2,1)}, u32[]{:S(2)}, u32[]{:S(2)}) collective-permute-start(bf16[192,1152]{1,0:T(8,128)(2,1)} %get-tuple-element.58), channel_id=1, source_target_pairs={{0,4},{2,6},{4,0},{6,2},{8,12},{10,14},{12,8},{14,10},{16,20},{18,... | collective-permute-start | bytes 1327112 | tf_op jit(solution)/shard_map/ppermute | solution.py:211
  91.4 30.9 %collective-permute-start.2 = (bf16[192,1152]{1,0:T(8,128)(2,1)S(1)}, bf16[192,1152]{1,0:T(8,128)(2,1)}, u32[]{:S(2)}, u32[]{:S(2)}) collective-permute-start(bf16[192,1152]{1,0:T(8,128)(2,1)S(1)} %collective-permute-done), channel_id=1, source_target_pairs={{8,0},{10,2},{12,4},{14,6},{16,8},{18,10},{20,12},{22,14},{24,16},... | collective-permute-start | bytes 1327112 | tf_op jit(solution)/shard_map/ppermute | solution.py:198
  92.7 21.6 %collective-permute-start.3 = (bf16[192,1152]{1,0:T(8,128)(2,1)S(1)}, bf16[192,1152]{1,0:T(8,128)(2,1)}, u32[]{:S(2)}, u32[]{:S(2)}) collective-permute-start(bf16[192,1152]{1,0:T(8,128)(2,1)S(1)} %collective-permute-done.1), channel_id=1, source_target_pairs={{0,8},{2,10},{4,12},{6,14},{8,16},{10,18},{12,20},{14,22},{16,24},... | collective-permute-start | bytes 1327112 | tf_op jit(solution)/shard_map/ppermute | solution.py:198
  104.6 54.4 %copy-start = (bf16[8,80,1024]{2,1,0:T(8,128)(2,1)}, bf16[8,80,1024]{2,1,0:T(8,128)(2,1)S(1)}, u32[]{:S(2)}) copy-start(bf16[8,80,1024]{2,1,0:T(8,128)(2,1)S(1)} %all-to-all-done.1.refs_2_.refs_0_) | copy-start | bytes 3932164
  104.6 38.3 %all-to-all-start.2 = ((bf16[8,64,1024]{2,1,0:T(8,128)(2,1)}), bf16[8,64,1024]{2,1,0:T(8,128)(2,1)}, u32[]{:S(2)}, u32[]{:S(2)}) async-start(bf16[8,64,1024]{2,1,0:T(8,128)(2,1)} %get-tuple-element.33), calls=%async_computation.2 | async-start | bytes 2097152 | tf_op jit(solution)/shard_map/all_to_all | solution.py:111
  108.8 32.4 %copy-start.11 = (s32[4,4]{1,0:T(4,128)S(1)}, s32[4,4]{1,0:T(4,128)}, u32[]{:S(2)}) copy-start(s32[4,4]{1,0:T(4,128)} %constant.126.clone) | copy-start | bytes 196
  108.9 34.0 %copy-start.5 = (bf16[192,1152]{1,0:T(8,128)(2,1)}, bf16[192,1152]{1,0:T(8,128)(2,1)S(1)}, u32[]{:S(2)}) copy-start(bf16[192,1152]{1,0:T(8,128)(2,1)S(1)} %broadcast_select_fusion.1) | copy-start | bytes 1327108
  108.9 44.9 %collective-permute-start.7 = (bf16[192,1152]{1,0:T(8,128)(2,1)S(1)}, bf16[192,1152]{1,0:T(8,128)(2,1)}, u32[]{:S(2)}, u32[]{:S(2)}) collective-permute-start(bf16[192,1152]{1,0:T(8,128)(2,1)S(1)} %broadcast_select_fusion.1), channel_id=1, source_target_pairs={{0,4},{2,6},{4,0},{6,2},{8,12},{10,14},{12,8},{14,10},{16,20},{18,... | collective-permute-start | bytes 1327112 | tf_op jit(solution)/shard_map/ppermute | solution.py:211
  114.4 24.5 %collective-permute-start.5 = (bf16[192,1152]{1,0:T(8,128)(2,1)}, bf16[192,1152]{1,0:T(8,128)(2,1)S(1)}, u32[]{:S(2)}, u32[]{:S(2)}) collective-permute-start(bf16[192,1152]{1,0:T(8,128)(2,1)} %collective-permute-done.3), channel_id=1, source_target_pairs={{0,8},{2,10},{4,12},{6,14},{8,16},{10,18},{12,20},{14,22},{16,24},... | collective-permute-start | bytes 1327112 | tf_op jit(solution)/shard_map/ppermute | solution.py:198
  122.4 16.5 %collective-permute-start.4 = (bf16[192,1152]{1,0:T(8,128)(2,1)}, bf16[192,1152]{1,0:T(8,128)(2,1)S(1)}, u32[]{:S(2)}, u32[]{:S(2)}) collective-permute-start(bf16[192,1152]{1,0:T(8,128)(2,1)} %collective-permute-done.2), channel_id=1, source_target_pairs={{8,0},{10,2},{12,4},{14,6},{16,8},{18,10},{20,12},{22,14},{24,16},... | collective-permute-start | bytes 1327112 | tf_op jit(solution)/shard_map/ppermute | solution.py:198
  124.8 29.1 %copy-start.6 = (bf16[192,1152]{1,0:T(8,128)(2,1)}, bf16[192,1152]{1,0:T(8,128)(2,1)S(1)}, u32[]{:S(2)}) copy-start(bf16[192,1152]{1,0:T(8,128)(2,1)S(1)} %broadcast_select_fusion) | copy-start | bytes 1327108
  124.8 29.1 %collective-permute-start.8 = (bf16[192,1152]{1,0:T(8,128)(2,1)S(1)}, bf16[192,1152]{1,0:T(8,128)(2,1)}, u32[]{:S(2)}, u32[]{:S(2)}) collective-permute-start(bf16[192,1152]{1,0:T(8,128)(2,1)S(1)} %broadcast_select_fusion), channel_id=1, source_target_pairs={{0,4},{2,6},{4,0},{6,2},{8,12},{10,14},{12,8},{14,10},{16,20},{18,... | collective-permute-start | bytes 1327112 | tf_op jit(solution)/shard_map/ppermute | solution.py:211
  139.7 14.2 %collective-permute-start.9 = (bf16[192,1152]{1,0:T(8,128)(2,1)}, bf16[192,1152]{1,0:T(8,128)(2,1)}, u32[]{:S(2)}, u32[]{:S(2)}) collective-permute-start(bf16[192,1152]{1,0:T(8,128)(2,1)} %select_select_fusion), channel_id=1, source_target_pairs={{0,4},{2,6},{4,0},{6,2},{8,12},{10,14},{12,8},{14,10},{16,20},{18,... | collective-permute-start | bytes 1327112 | tf_op jit(solution)/shard_map/ppermute | solution.py:211
  141.3 43.3 %collective-permute-start.11 = (bf16[8,112,1024]{2,1,0:T(8,128)(2,1)}, bf16[8,112,1024]{2,1,0:T(8,128)(2,1)}, u32[]{:S(2)}, u32[]{:S(2)}) collective-permute-start(bf16[8,112,1024]{2,1,0:T(8,128)(2,1)} %all-to-all-done.refs_0_), channel_id=1, source_target_pairs={{0,2},{2,0},{4,6},{6,4},{8,10},{10,8},{12,14},{14,12},{16,18},{18,... | collective-permute-start | bytes 5505032 | tf_op jit(solution)/shard_map/ppermute | solution.py:117
  142.9 75.2 %all-to-all-start.3 = ((bf16[8,64,1024]{2,1,0:T(8,128)(2,1)}), bf16[8,64,1024]{2,1,0:T(8,128)(2,1)S(1)}, u32[]{:S(2)}, u32[]{:S(2)}) async-start(bf16[8,64,1024]{2,1,0:T(8,128)(2,1)} %get-tuple-element.35), calls=%async_computation.3 | async-start | bytes 2097152 | tf_op jit(solution)/shard_map/all_to_all | solution.py:111
  153.9 5.7 %copy-start.13 = (s32[16]{0:T(128)S(1)}, s32[16]{0:T(128)}, u32[]{:S(2)}) copy-start(s32[16]{0:T(128)} %constant.128.clone) | copy-start | bytes 196
  153.9 5.7 %copy-start.14 = (s32[16]{0:T(128)S(1)}, s32[16]{0:T(128)}, u32[]{:S(2)}) copy-start(s32[16]{0:T(128)} %constant.131) | copy-start | bytes 196
  159.0 6.6 %collective-permute-start.10 = (bf16[768,1024]{1,0:T(8,128)(2,1)}, bf16[768,1024]{1,0:T(8,128)(2,1)}, u32[]{:S(2)}, u32[]{:S(2)}) collective-permute-start(bf16[768,1024]{1,0:T(8,128)(2,1)} %bitcast.53), channel_id=1, source_target_pairs={{0,1},{1,0},{2,3},{3,2},{4,5},{5,4},{6,7},{7,6},{8,9},{9,8},{10,11... | collective-permute-start | bytes 4718600 | tf_op jit(solution)/shard_map/ppermute | solution.py:130
  159.0 53.7 %collective-permute-start.12 = (bf16[8,80,1024]{2,1,0:T(8,128)(2,1)S(1)}, bf16[8,80,1024]{2,1,0:T(8,128)(2,1)}, u32[]{:S(2)}, u32[]{:S(2)}) collective-permute-start(bf16[8,80,1024]{2,1,0:T(8,128)(2,1)S(1)} %all-to-all-done.1.refs_2_.refs_0_), channel_id=1, source_target_pairs={{0,2},{2,0},{4,6},{6,4},{8,10},{10,8},{12,14},{14,12},{16,18},{18,... | collective-permute-start | bytes 3932168 | tf_op jit(solution)/shard_map/ppermute | solution.py:117
  160.1 76.6 %collective-permute-start.13 = (bf16[8,64,1024]{2,1,0:T(8,128)(2,1)}, bf16[8,64,1024]{2,1,0:T(8,128)(2,1)}, u32[]{:S(2)}, u32[]{:S(2)}) collective-permute-start(bf16[8,64,1024]{2,1,0:T(8,128)(2,1)} %all-to-all-done.2.refs_2_), channel_id=1, source_target_pairs={{0,2},{2,0},{4,6},{6,4},{8,10},{10,8},{12,14},{14,12},{16,18},{18,... | collective-permute-start | bytes 3145736 | tf_op jit(solution)/shard_map/ppermute | solution.py:117
  218.1 35.9 %copy-start.1 = (bf16[8,64,1024]{2,1,0:T(8,128)(2,1)}, bf16[8,64,1024]{2,1,0:T(8,128)(2,1)S(1)}, u32[]{:S(2)}) copy-start(bf16[8,64,1024]{2,1,0:T(8,128)(2,1)S(1)} %all-to-all-done.3.refs_0_) | copy-start | bytes 3145732
  218.1 32.8 %all-to-all-start.4 = ((bf16[8,64,1024]{2,1,0:T(8,128)(2,1)}), bf16[8,64,1024]{2,1,0:T(8,128)(2,1)S(1)}, u32[]{:S(2)}, u32[]{:S(2)}) async-start(bf16[8,64,1024]{2,1,0:T(8,128)(2,1)} %get-tuple-element.37), calls=%async_computation.4 | async-start | bytes 2097152 | tf_op jit(solution)/shard_map/all_to_all | solution.py:111
  250.9 4.6 %copy-start.2 = (bf16[8,64,1024]{2,1,0:T(8,128)(2,1)}, bf16[8,64,1024]{2,1,0:T(8,128)(2,1)S(1)}, u32[]{:S(2)}) copy-start(bf16[8,64,1024]{2,1,0:T(8,128)(2,1)S(1)} %all-to-all-done.4.refs_2_) | copy-start | bytes 3145732
  250.9 1.4 copy-start.8
  250.9 1.9 copy-start.15
  253.8 3.2 collective-permute-start.14
  253.9 26.2 %collective-permute-start.15 = (bf16[8,64,1024]{2,1,0:T(8,128)(2,1)S(1)}, bf16[8,64,1024]{2,1,0:T(8,128)(2,1)}, u32[]{:S(2)}, u32[]{:S(2)}) collective-permute-start(bf16[8,64,1024]{2,1,0:T(8,128)(2,1)S(1)} %all-to-all-done.3.refs_0_), channel_id=1, source_target_pairs={{0,2},{2,0},{4,6},{6,4},{8,10},{10,8},{12,14},{14,12},{16,18},{18,... | collective-permute-start | bytes 3145736 | tf_op jit(solution)/shard_map/ppermute | solution.py:117
  255.5 46.6 %collective-permute-start.16 = (bf16[8,64,1024]{2,1,0:T(8,128)(2,1)S(1)}, bf16[8,64,1024]{2,1,0:T(8,128)(2,1)}, u32[]{:S(2)}, u32[]{:S(2)}) collective-permute-start(bf16[8,64,1024]{2,1,0:T(8,128)(2,1)S(1)} %all-to-all-done.4.refs_2_), channel_id=1, source_target_pairs={{0,2},{2,0},{4,6},{6,4},{8,10},{10,8},{12,14},{14,12},{16,18},{18,... | collective-permute-start | bytes 3145736 | tf_op jit(solution)/shard_map/ppermute | solution.py:117
  258.2 50.3 %all-to-all-start.5 = ((bf16[8,96,512]{2,1,0:T(8,128)(2,1)}), bf16[8,96,512]{2,1,0:T(8,128)(2,1)S(1)}, u32[]{:S(2)}, u32[]{:S(2)}) async-start(bf16[8,96,512]{2,1,0:T(8,128)(2,1)} %bitcast.60), calls=%async_computation.5 | async-start | bytes 1572864 | tf_op jit(solution)/shard_map/all_to_all | solution.py:111
  264.2 39.0 %copy-start.16 = (bf16[768,1024]{1,0:T(8,128)(2,1)S(1)}, bf16[768,1024]{1,0:T(8,128)(2,1)}, u32[]{:S(2)}) copy-start(bf16[768,1024]{1,0:T(8,128)(2,1)} %multiply_convert_fusion.1) | copy-start | bytes 4718596
  304.2 3.2 collective-permute-start.17
  304.6 1.7 copy-start.17
  307.3 7.5 %copy-start.12 = (f32[192,2]{0,1:T(2,128)S(1)}, f32[192,2]{0,1:T(2,128)}, u32[]{:S(2)}) copy-start(f32[192,2]{0,1:T(2,128)} %param.12) | copy-start | bytes 4612
  308.4 26.8 %all-to-all-start.6 = ((bf16[8,96,512]{2,1,0:T(8,128)(2,1)}), bf16[8,96,512]{2,1,0:T(8,128)(2,1)S(1)}, u32[]{:S(2)}, u32[]{:S(2)}) async-start(bf16[8,96,512]{2,1,0:T(8,128)(2,1)} %bitcast.26), calls=%async_computation.6 | async-start | bytes 1572864 | tf_op jit(solution)/shard_map/all_to_all | solution.py:111
  337.1 4.4 %collective-permute-start.18 = (bf16[192,1024]{1,0:T(8,128)(2,1)S(1)}, bf16[192,1024]{1,0:T(8,128)(2,1)S(1)}, u32[]{:S(2)}, u32[]{:S(2)}) collective-permute-start(bf16[192,1024]{1,0:T(8,128)(2,1)S(1)} %fusion.2), channel_id=1, source_target_pairs={{0,1},{1,0},{2,3},{3,2},{4,5},{5,4},{6,7},{7,6},{8,9},{9,8},{10,11... | collective-permute-start | bytes 1179656 | tf_op jit(solution)/shard_map/ppermute | solution.py:130
  341.5 0.9 copy-start.7
